TPU v7x, 32 devices: a whole 2x2x4 slice. The times are simulated.
32 devices in a mesh: ep: 8 (over z, x), tp: 4 (over y, core).
Axes of the slice: x: 2, y: 2, z: 4, core: 2. Of those that a mesh axis runs over, the one named last changes fastest.
Arguments:
- query_latent: bfloat16 [2048, 768], P('ep'), may hold values from -600 to 600
- shared_latent: bfloat16 [2048, 512], P('ep'), may hold values from -600 to 600
- rotary_key: bfloat16 [2048, 64], P('ep'), may hold values from -2500 to 2500
- query_gain: float32 [768], replicated, may hold values from 0.1 to 1.9
- shared_gain: float32 [512], replicated, may hold values from 0.1 to 1.9
- query_plain_weight: bfloat16 [768, 2048], P(None, 'tp'), may hold values from -0.21875 to 0.21875
- query_turn_weight: bfloat16 [768, 1024], P(None, 'tp'), may hold values from -0.21875 to 0.21875
- key_weight: bfloat16 [512, 2048], P(None, 'tp'), may hold values from -0.25 to 0.25
- value_weight: bfloat16 [512, 2048], P(None, 'tp'), may hold values from -0.25 to 0.25
- mixer_out_weight: bfloat16 [2048, 2048], P('tp'), may hold values from -1 to 1
- expert_input: bfloat16 [1024, 2048], P('ep'), may hold values from -600 to 600
- expert_gain: float32 [2048], replicated, may hold values from 0.1 to 1.9
- routing: int32 [1024, 4], P('ep'), may hold values from 0 to 7, all different within a row; in each aligned block of 128 rows (0 to 127, 128 to 255, ...) at most 85 rows name the same one
- routing_weight: float32 [1024, 4], P('ep'), may hold values from 0.05 to 1
- gate_weight: bfloat16 [8, 2048, 2048], P('ep', None, 'tp'), may hold values from -0.375 to 0.375
- up_weight: bfloat16 [8, 2048, 2048], P('ep', None, 'tp'), may hold values from -0.375 to 0.375
- down_weight: bfloat16 [8, 2048, 2048], P('ep', 'tp'), may hold values from -0.01953125 to 0.01953125
Outputs:
- mixer_output: bfloat16 [2048, 2048], P('ep')
- expert_output: bfloat16 [1024, 2048], P('ep')
Inputs may be any that keep to these rules, and one draw needn't show every extreme that they name: `routing`: each row names 4 different experts. In each aligned block of 128 rows (the rows of one index of ep) no expert is named by more than 85 rows, and in some block some expert is named by exactly 85.
All inputs are finite; a program needn't handle non-finite values.
Results may differ from a plain program's by a relative error of at most 0.019.
Values may be sent and summed in bfloat16 or wider, within the bound.
A program may use at most 128 MiB of HBM per device.

v0:
```python
import functools

import jax
import jax.numpy as jnp
from jax import lax
from jax.experimental import pallas as pl
from jax.experimental.pallas import tpu as pltpu
from jax.sharding import PartitionSpec as P

NOPE = 128
ROPE = 64
VDIM = 128
LANES = 128
CORES = 2

EPSILON = 1e-06
CLAMP_LIMIT = 7.0
SLOPE = 1.702
ROTARY_BASE = 10000.0
NEGATIVE = -1e30
VMEM_LIMIT = 60 * 1024 * 1024
F32 = jnp.float32
BF16 = jnp.bfloat16


def norm_scale(values):
    widened = values.astype(F32)
    return widened * lax.rsqrt(jnp.mean(widened * widened, axis=-1, keepdims=True) + EPSILON)


def norm_rows(values, gains):
    return (norm_scale(values) * gains).astype(BF16)


def rotate_heads(values, position):
    half = ROPE // 2
    lane = jnp.arange(values.shape[-1], dtype=jnp.int32)
    frequency = ROTARY_BASE ** (-2.0 * (lane % half).astype(F32) / ROPE)
    angles = position.astype(F32)[:, None] * frequency[None, :]
    upper = (lane % ROPE >= half)[None, :]
    swapped = jnp.where(upper, jnp.roll(values, half, axis=1), -jnp.roll(values, -half, axis=1))
    return values * jnp.cos(angles) + swapped * jnp.sin(angles)


def remote(src, dst, send_sem, recv_sem, ep, tp):
    return pltpu.make_async_remote_copy(
        src_ref=src,
        dst_ref=dst,
        send_sem=send_sem,
        recv_sem=recv_sem,
        device_id=(ep, tp),
        device_id_type=pl.DeviceIdType.MESH,
    )


def enter(n_ep, n_tp, me_e, me_t):
    barrier = pltpu.get_barrier_semaphore()
    for d in range(1, n_ep):
        pl.semaphore_signal(
            barrier,
            inc=1,
            device_id=(lax.rem(me_e + d, n_ep), me_t),
            device_id_type=pl.DeviceIdType.MESH,
        )
    for k in range(1, n_tp):
        pl.semaphore_signal(
            barrier,
            inc=1,
            device_id=(me_e, lax.rem(me_t + k, n_tp)),
            device_id_type=pl.DeviceIdType.MESH,
        )
    pl.semaphore_wait(barrier, n_ep - 1 + n_tp - 1)


def gather_kernel(
    n_ep,
    n_tp,
    heads,
    lat,
    disp,
    queries,
    key_w,
    value_w,
    mixer_w,
    arr,
    mpart,
    lat_all,
    out,
    keys,
    values,
    loc_sem,
    ep_s,
    ep_r,
    y_s,
    y_r,
    c_s,
    c_r,
):
    me_e = lax.axis_index("ep")
    me_t = lax.axis_index("tp")
    n_y = n_tp // CORES
    y = me_t // CORES
    c = lax.rem(me_t, CORES)
    mate = y * CORES + (1 - c)
    width = disp.shape[2]

    def place(j, e, t):
        if j == 0:
            return lat_all.at[e, t]
        return arr.at[e, :, pl.ds(pl.multiple_of(t * width, LANES), width)]

    local = []
    for j in range(2):
        copy = pltpu.make_async_copy(
            lat if j == 0 else disp.at[me_e], place(j, me_e, me_t), loc_sem.at[j]
        )
        copy.start()
        local.append(copy)
    enter(n_ep, n_tp, me_e, me_t)
    sends = []
    for j in range(2):
        for d in range(1, n_ep):
            peer = lax.rem(me_e + d, n_ep)
            copy = remote(
                lat if j == 0 else disp.at[peer],
                place(j, me_e, me_t),
                ep_s.at[d, j],
                ep_r.at[d, j],
                peer,
                me_t,
            )
            copy.start()
            sends.append(copy)

    def relay(j, d):
        src = lax.rem(me_e - d + n_ep, n_ep)
        here = place(j, src, me_t)
        if d == 0:
            local[j].wait()
        else:
            remote(here, here, ep_s.at[d, j], ep_r.at[d, j], src, me_t).wait_recv()
        for k in range(1, n_y):
            to = lax.rem(y + k, n_y) * CORES + c
            copy = remote(here, here, y_s.at[d, k, j], y_r.at[d, k, j], me_e, to)
            copy.start()
            sends.append(copy)
        copy = remote(here, here, c_s.at[d, 0, j], c_r.at[d, 0, j], me_e, mate)
        copy.start()
        sends.append(copy)

    def forward(j, d):
        src = lax.rem(me_e - d + n_ep, n_ep)
        for k in range(1, n_y):
            got = place(j, src, lax.rem(y - k + n_y, n_y) * CORES + c)
            remote(got, got, y_s.at[d, k, j], y_r.at[d, k, j], me_e, me_t).wait_recv()
            copy = remote(got, got, c_s.at[d, k, j], c_r.at[d, k, j], me_e, mate)
            copy.start()
            sends.append(copy)

    def arrive(j, d):
        src = lax.rem(me_e - d + n_ep, n_ep)
        for k in range(n_y):
            got = place(j, src, lax.rem(y - k + n_y, n_y) * CORES + (1 - c))
            remote(got, got, c_s.at[d, k, j], c_r.at[d, k, j], me_e, mate).wait_recv()

    for d in range(n_ep):
        relay(0, d)
        if d > 0:
            forward(0, d - 1)
    relay(1, 0)
    forward(0, n_ep - 1)
    for d in range(n_ep):
        arrive(0, d)
        if d % 2 == 1 and d // 2 + 1 < n_ep // 2:
            relay(1, d // 2 + 1)
        project(
            lax.rem(me_e - d + n_ep, n_ep), n_tp, heads, lat_all, key_w, value_w, keys, values
        )
    done = n_ep // 2
    for h in range(heads):
        attend(h, me_e, queries, keys, values, out)
        until = n_ep if h == heads - 1 else n_ep // 2 + (h + 1) * (n_ep // 2) // heads
        for d in range(done, until):
            relay(1, d)
        done = until
    mpart[...] = jnp.dot(out[...], mixer_w[...], preferred_element_type=F32).astype(BF16)
    for d in range(n_ep):
        forward(1, d)
    for d in range(n_ep):
        arrive(1, d)
    for copy in sends:
        copy.wait_send()


def project(e, n_tp, heads, lat_all, key_w, value_w, keys, values):
    share = lat_all.shape[2]
    rows = n_tp * share
    rank = key_w.shape[0]
    head_keys = NOPE + LANES
    at = pl.ds(pl.multiple_of(e * rows, rows), rows)
    block = lat_all[e].reshape(rows, rank + LANES)
    latent = block[:, :rank]
    k = jnp.dot(latent, key_w[...], preferred_element_type=F32).astype(BF16)
    values[at, :] = jnp.dot(latent, value_w[...], preferred_element_type=F32).astype(BF16)
    for h in range(heads):
        keys[at, h * head_keys : h * head_keys + NOPE] = k[:, h * NOPE : (h + 1) * NOPE]
        keys[at, h * head_keys + NOPE : (h + 1) * head_keys] = block[:, rank:]


def attend(h, me_e, queries, keys, values, out):
    rows = queries.shape[0]
    total = keys.shape[0]
    head_keys = NOPE + LANES
    row = lax.broadcasted_iota(jnp.int32, (rows, total), 0) + me_e * rows
    visible = lax.broadcasted_iota(jnp.int32, (rows, total), 1) <= row
    scaling = (NOPE + ROPE) ** (-0.5)
    cols = slice(h * head_keys, (h + 1) * head_keys)
    scores = lax.dot_general(
        queries[:, cols], keys[:, cols], (((1,), (1,)), ((), ())), preferred_element_type=F32
    )
    scores = jnp.where(visible, scores * scaling, NEGATIVE)
    weight = jnp.exp(scores - jnp.max(scores, axis=-1, keepdims=True))
    sums = jnp.sum(weight, axis=-1, keepdims=True)
    mixed = jnp.dot(
        weight.astype(BF16), values[:, h * VDIM : (h + 1) * VDIM], preferred_element_type=F32
    )
    out[:, h * VDIM : (h + 1) * VDIM] = (mixed / sums).astype(BF16)


def return_kernel(
    n_ep,
    n_tp,
    arrived,
    gate_hbm,
    up_hbm,
    down_hbm,
    mix,
    mpart,
    eout,
    mout,
    gate_w,
    up_w,
    down_w,
    load_sem,
    part,
    ca,
    sums,
    ya,
    res,
    ret,
    mca,
    msums,
    mya,
    ca_s,
    ca_r,
    ya_s,
    ya_r,
    ep_s,
    ep_r,
    oy_s,
    oy_r,
    oc_s,
    oc_r,
):
    me_e = lax.axis_index("ep")
    me_t = lax.axis_index("tp")
    n_y = n_tp // CORES
    y = me_t // CORES
    c = lax.rem(me_t, CORES)
    mate = y * CORES + (1 - c)
    width = res.shape[2]
    capacity = res.shape[1]
    pairs = n_ep // 2
    parity = lax.rem(me_e, 2)
    loads = []
    for n, (src, dst) in enumerate(((gate_hbm, gate_w), (up_hbm, up_w), (down_hbm, down_w))):
        copy = pltpu.make_async_copy(src.at[0], dst, load_sem.at[n])
        copy.start()
        loads.append(copy)

    def twin(i):
        return parity if i % 2 == 0 else 1 - parity

    def dest(i):
        return lax.rem(me_e // 2 + i // 2, pairs) * 2 + twin(i)

    def source(i):
        return lax.rem(me_e // 2 - i // 2 + pairs, pairs) * 2 + twin(i)

    def cols(t):
        return pl.ds(pl.multiple_of(t * width, LANES), width)

    def part_at(i, t):
        if i == n_ep:
            return mpart.at[:, cols(t)]
        return part.at[dest(i), :, cols(t)]

    def part_load(i, t):
        if i == n_ep:
            return mpart[:, cols(t)].astype(F32)
        return part[dest(i), :, cols(t)].astype(F32)

    enter(n_ep, n_tp, me_e, me_t)
    sends = []

    def go(copy):
        copy.start()
        sends.append(copy)

    def core_copy(i, k):
        dst = mca.at[k] if i == n_ep else ca.at[i, k]
        return remote(
            part_at(i, lax.rem(y + k, n_y) * CORES + (1 - c)),
            dst,
            ca_s.at[i, k],
            ca_r.at[i, k],
            me_e,
            mate,
        )

    def y_copy(i, k):
        src, dst = (msums, mya) if i == n_ep else (sums.at[i], ya.at[i])
        to = lax.rem(y + k, n_y) * CORES + c
        return remote(src.at[k - 1], dst.at[k - 1], ya_s.at[i, k], ya_r.at[i, k], me_e, to)

    def core_step(i):
        for k in list(range(1, n_y)) + [0]:
            go(core_copy(i, k))

    def y_step(i):
        for k in range(1, n_y):
            core_copy(i, k).wait_recv()
            got = (mca[k] if i == n_ep else ca[i, k]).astype(F32)
            value = (got + part_load(i, lax.rem(y + k, n_y) * CORES + c)).astype(BF16)
            if i == n_ep:
                msums[k - 1] = value
            else:
                sums[i, k - 1] = value
            go(y_copy(i, k))

    def ep_copy(i, e):
        return remote(res.at[i], ret.at[i], ep_s.at[i], ep_r.at[i], e, me_t)

    def sum_step(i):
        core_copy(i, 0).wait_recv()
        value = (mca[0] if i == n_ep else ca[i, 0]).astype(F32) + part_load(i, me_t)
        for k in range(1, n_y):
            y_copy(i, k).wait_recv()
            value = value + (mya[k - 1] if i == n_ep else ya[i, k - 1]).astype(F32)
        if i == n_ep:
            mout[:, cols(me_t)] = value.astype(BF16)
        elif i == 0:
            ret[0] = value.astype(BF16)
        else:
            res[i] = value.astype(BF16)
            go(ep_copy(i, dest(i)))

    def expert_step(s):
        base = lax.rem(me_e // 2 + s, pairs) * 2
        rows = arrived[pl.ds(pl.multiple_of(base * capacity, 2 * capacity), 2 * capacity), :]
        if s == 1 % pairs:
            loads[0].wait()
            loads[1].wait()
        gate = jnp.minimum(jnp.dot(rows, gate_w[...], preferred_element_type=F32), CLAMP_LIMIT)
        up = jnp.clip(
            jnp.dot(rows, up_w[...], preferred_element_type=F32), -CLAMP_LIMIT, CLAMP_LIMIT
        )
        hidden = ((up + 1.0) * (gate * jax.nn.sigmoid(SLOPE * gate))).astype(BF16)
        if s == 1 % pairs:
            loads[2].wait()
        value = jnp.dot(hidden, down_w[...], preferred_element_type=F32)
        part[base] = value[:capacity].astype(BF16)
        part[base + 1] = value[capacity:].astype(BF16)

    def out_copy(j, k, t, to, sem_s, sem_r):
        ref = (mout if j == 0 else eout).at[:, cols(t)]
        return remote(ref, ref, sem_s.at[j, k], sem_r.at[j, k], me_e, to)

    def out_send(j):
        for k in range(1, n_y):
            go(out_copy(j, k, me_t, lax.rem(y + k, n_y) * CORES + c, oy_s, oy_r))
        go(out_copy(j, 0, me_t, mate, oc_s, oc_r))

    core_step(n_ep)
    turns = [n % pairs for n in range(1, pairs + 1)]
    for n, turn in enumerate(turns):
        expert_step(turn)
        for i in (2 * turn, 2 * turn + 1):
            core_step(i)
        if n == 0:
            y_step(n_ep)
        for i in (2 * turn, 2 * turn + 1):
            y_step(i)
        if n > 0:
            for i in (2 * turns[n - 1], 2 * turns[n - 1] + 1):
                sum_step(i)
    sum_step(n_ep)
    out_send(0)
    for i in (1, 0):
        sum_step(i)
    acc = None
    for i in [0] + list(range(2, n_ep)) + [1]:
        if i > 0:
            ep_copy(i, source(i)).wait_recv()
        mixing = mix[source(i)]
        high = mixing.astype(BF16)
        low = (mixing - high.astype(F32)).astype(BF16)
        rows = ret[i]
        term = jnp.dot(high, rows, preferred_element_type=F32) + jnp.dot(
            low, rows, preferred_element_type=F32
        )
        acc = term if acc is None else acc + term
    eout[:, cols(me_t)] = acc.astype(BF16)
    out_send(1)
    for j in range(2):
        for k in range(1, n_y):
            t = lax.rem(y - k + n_y, n_y) * CORES + c
            out_copy(j, k, t, me_t, oy_s, oy_r).wait_recv()
            go(out_copy(j, k, t, mate, oc_s, oc_r))
    for j in range(2):
        for k in range(n_y):
            t = lax.rem(y - k + n_y, n_y) * CORES + (1 - c)
            out_copy(j, k, t, mate, oc_s, oc_r).wait_recv()
    for copy in sends:
        copy.wait_send()


def vmem(count):
    return [pl.BlockSpec(memory_space=pltpu.VMEM)] * count


def per_device(
    n_ep,
    n_tp,
    query_latent,
    shared_latent,
    rotary_key,
    query_gain,
    shared_gain,
    query_plain_weight,
    query_turn_weight,
    key_weight,
    value_weight,
    mixer_out_weight,
    expert_input,
    expert_gain,
    routing,
    routing_weight,
    gate_weight,
    up_weight,
    down_weight,
):
    me_e = lax.axis_index("ep")
    me_t = lax.axis_index("tp")
    n_y = n_tp // CORES
    row_count = query_latent.shape[0]
    heads = query_plain_weight.shape[1] // NOPE
    rank = shared_latent.shape[1]

    share = row_count // n_tp
    first = me_t * share
    lat = norm_rows(lax.dynamic_slice_in_dim(shared_latent, first, share, 0), shared_gain)
    own_position = me_e * row_count + first + jnp.arange(share, dtype=jnp.int32)
    turned = rotate_heads(
        lax.dynamic_slice_in_dim(rotary_key, first, share, 0).astype(F32), own_position
    ).astype(BF16)
    lat = jnp.concatenate([lat, turned, jnp.zeros((share, LANES - ROPE), BF16)], axis=1)

    token_count, width = expert_input.shape
    top_count = routing.shape[1]
    capacity = 4 * token_count * top_count // (3 * n_ep)
    capacity = -(-capacity // 8) * 8
    part_width = width // n_tp
    normed = norm_rows(expert_input, expert_gain)
    normed = lax.dynamic_slice_in_dim(normed, me_t * part_width, part_width, 1)
    flattened = routing.reshape(token_count * top_count)
    matches = flattened[:, None] == jnp.arange(n_ep, dtype=jnp.int32)[None, :]
    count = token_count * top_count
    lower = jnp.arange(count)[:, None] > jnp.arange(count)[None, :]
    ranking = jnp.dot(
        lower.astype(BF16), matches.astype(BF16), preferred_element_type=F32
    ).astype(jnp.int32)
    slot_index = jnp.sum(jnp.where(matches, ranking, 0), axis=1)
    target = (flattened * capacity + slot_index).reshape(token_count, top_count)
    slot_ids = jnp.arange(n_ep * capacity, dtype=jnp.int32)
    table = jnp.zeros((n_ep * capacity, token_count), jnp.bool_)
    mixing = jnp.zeros((token_count, n_ep * capacity), F32)
    for k in range(top_count):
        table = table | (target[:, k][None, :] == slot_ids[:, None])
        mixing = mixing + jnp.where(
            target[:, k][:, None] == slot_ids[None, :], routing_weight[:, k][:, None], 0.0
        )
    disp = jnp.dot(table.astype(BF16), normed, preferred_element_type=F32).astype(BF16)
    disp = disp.reshape(n_ep, capacity, part_width)
    mixing = jnp.transpose(mixing.reshape(token_count, n_ep, capacity), (1, 0, 2))

    position = me_e * row_count + jnp.arange(row_count, dtype=jnp.int32)
    query_normed = norm_rows(query_latent, query_gain)
    query_plain = jnp.dot(query_normed, query_plain_weight, preferred_element_type=F32)
    query_plain = query_plain.astype(BF16)
    query_raw = jnp.dot(query_normed, query_turn_weight, preferred_element_type=F32)
    query_turned = rotate_heads(query_raw, position).astype(BF16)
    blank = jnp.zeros((row_count, LANES - ROPE), BF16)
    pieces = []
    for h in range(heads):
        pieces.append(query_plain[:, h * NOPE : (h + 1) * NOPE])
        pieces.append(query_turned[:, h * ROPE : (h + 1) * ROPE])
        pieces.append(blank)
    queries = jnp.concatenate(pieces, axis=1)
    total = n_ep * row_count
    dma = pltpu.SemaphoreType.DMA
    arrived, mixer_partial = pl.pallas_call(
        functools.partial(gather_kernel, n_ep, n_tp, heads),
        out_shape=(
            jax.ShapeDtypeStruct((n_ep, capacity, width), BF16),
            jax.ShapeDtypeStruct((row_count, width), BF16),
        ),
        in_specs=vmem(6),
        out_specs=vmem(2),
        scratch_shapes=[
            pltpu.VMEM((n_ep, n_tp, share, rank + LANES), BF16),
            pltpu.VMEM((row_count, heads * VDIM), BF16),
            pltpu.VMEM((total, heads * (NOPE + LANES)), BF16),
            pltpu.VMEM((total, heads * VDIM), BF16),
            dma((2,)),
            dma((n_ep, 2)),
            dma((n_ep, 2)),
            dma((n_ep, n_y, 2)),
            dma((n_ep, n_y, 2)),
            dma((n_ep, n_y, 2)),
            dma((n_ep, n_y, 2)),
        ],
        compiler_params=pltpu.CompilerParams(
            collective_id=0, has_side_effects=True, vmem_limit_bytes=VMEM_LIMIT
        ),
    )(lat, disp, queries, key_weight, value_weight, mixer_out_weight)
    arrived = arrived.reshape(n_ep * capacity, width)
    units = gate_weight.shape[2]

    expert_output, mixer_output = pl.pallas_call(
        functools.partial(return_kernel, n_ep, n_tp),
        out_shape=(
            jax.ShapeDtypeStruct((token_count, width), BF16),
            jax.ShapeDtypeStruct((row_count, width), BF16),
        ),
        in_specs=vmem(1) + [pl.BlockSpec(memory_space=pl.ANY)] * 3 + vmem(2),
        out_specs=vmem(2),
        scratch_shapes=[
            pltpu.VMEM((width, units), BF16),
            pltpu.VMEM((width, units), BF16),
            pltpu.VMEM((units, width), BF16),
            dma((3,)),
            pltpu.VMEM((n_ep, capacity, width), BF16),
            pltpu.VMEM((n_ep, n_y, capacity, part_width), BF16),
            pltpu.VMEM((n_ep, n_y - 1, capacity, part_width), BF16),
            pltpu.VMEM((n_ep, n_y - 1, capacity, part_width), BF16),
            pltpu.VMEM((n_ep, capacity, part_width), BF16),
            pltpu.VMEM((n_ep, capacity, part_width), BF16),
            pltpu.VMEM((n_y, row_count, part_width), BF16),
            pltpu.VMEM((n_y - 1, row_count, part_width), BF16),
            pltpu.VMEM((n_y - 1, row_count, part_width), BF16),
            dma((n_ep + 1, n_y)),
            dma((n_ep + 1, n_y)),
            dma((n_ep + 1, n_y)),
            dma((n_ep + 1, n_y)),
            dma((n_ep,)),
            dma((n_ep,)),
            dma((2, n_y)),
            dma((2, n_y)),
            dma((2, n_y)),
            dma((2, n_y)),
        ],
        compiler_params=pltpu.CompilerParams(
            collective_id=1, has_side_effects=True, vmem_limit_bytes=VMEM_LIMIT
        ),
    )(arrived, gate_weight, up_weight, down_weight, mixing, mixer_partial)
    return (mixer_output, expert_output)


def solution(mesh):
    return jax.shard_map(
        functools.partial(per_device, mesh.shape["ep"], mesh.shape["tp"]),
        mesh=mesh,
        in_specs=(
            P("ep", None),
            P("ep", None),
            P("ep", None),
            P(),
            P(),
            P(None, "tp"),
            P(None, "tp"),
            P(None, "tp"),
            P(None, "tp"),
            P("tp", None),
            P("ep", None),
            P(),
            P("ep", None),
            P("ep", None),
            P("ep", None, "tp"),
            P("ep", None, "tp"),
            P("ep", "tp", None),
        ),
        out_specs=(P("ep", None), P("ep", None)),
        check_vma=False,
    )
```

profile of v0, /device:TPU:0, one launch (start us, length us, event | category | flops | bytes accessed | tf_op | source)
XLA Modules:
  0.0 119.4 jit_solution(8119308641024355975)
XLA Ops:
  0.7 1.1 fusion.19
  1.8 1.2 %multiply_reduce_fusion = f32[128]{0:T(128)S(1)} fusion(bf16[128,2048]{1,0:T(8,128)(2,1)} %param.27), kind=kLoop, calls=%fused_computation.5 | loop fusion | flops 786304 | bytes 524800 | tf_op jit(solution)/shard_map/reduce_sum | solution.py:28
  3.1 1.2 fusion.2
  4.3 0.8 dynamic-slice
  5.1 0.8 slice_bitcast_fusion.3
  5.9 0.8 constant_dynamic-slice_fusion
  6.8 0.9 fusion.21
  7.8 0.8 copy.44
  8.7 0.3 fusion.1
  9.1 0.7 multiply_add_fusion.1
  9.9 0.2 fusion.30
  10.1 0.7 maximum_maximum_fusion.lat
  10.8 0.3 fusion.25
  11.1 0.4 convolution_convert_fusion.1
  11.7 1.1 select_add_fusion.mix
  12.8 0.1 fusion.43
  12.9 1.2 %fusion.11 = bf16[256,256]{1,0:T(8,128)(2,1)S(1)} fusion(f32[256,256]{1,0:T(8,128)S(1)} %fusion.25, f32[256,224]{1,0:T(8,128)S(1)} %get-tuple-element.15, f32[256,32]{1,0:T(8,128)S(1)} %get-tuple-element.17, f32[256,32]{1,0:T(8,128)S(1)} %get-tuple-element.16, f32[256,224]{1,0:T(8,128)S(1)} %get-tuple-element.14, f32[256]{0:T(256)S(1)} %fusion.35, ...), kind=kLoop, calls=%fused_computation.24 | loop fusion | flops 589824 | bytes 919808 | tf_op jit(solution)/shard_map/convert_element_type | solution.py:502
  14.1 0.1 fusion.45
  14.3 1.1 concatenate.24.queries
  15.4 1.3 %convolution_convert_fusion = bf16[704,512]{1,0:T(8,128)(2,1)} fusion(s32[128]{0:T(128)S(1)} %get-tuple-element.29, s32[128]{0:T(128)S(1)} %get-tuple-element.30, s32[128]{0:T(128)S(1)} %get-tuple-element.31, s32[128]{0:T(128)S(1)} %get-tuple-element.28, f32[128,2048]{1,0:T(8,128)S(1)} %convert_element_type.74, s32[]{:T(128)S(6)} %select_n.82, ...), kind=kOutput, calls=%fused_computation | convolution fusion | flops 93462528 | bytes 987652 | tf_op jit(solution)/shard_map/dot_general | solution.py:493
  16.7 50.2 %shard_map.176 = (bf16[8,88,2048]{2,1,0:T(8,128)(2,1)}, bf16[256,2048]{1,0:T(8,128)(2,1)}) custom-call(bf16[64,640]{1,0:T(8,128)(2,1)} %maximum_maximum_fusion.lat, bf16[8,88,512]{2,1,0:T(8,128)(2,1)} %bitcast.20, bf16[256,1024]{1,0:T(8,128)(2,1)} %concatenate.24.queries, bf16[512,512]{1,0:T(8,128)(2,1)} %key_w.1, bf16[512,512]{1,0:T(8,128)(2,1)} %value_w.1, ...), custom_call_target="tpu_custom_call" | custom-call | tf_op jit(solution)/shard_map/pallas_call | solution.py:512
  66.9 49.3 %shard_map.177 = (bf16[128,2048]{1,0:T(8,128)(2,1)}, bf16[256,2048]{1,0:T(8,128)(2,1)}) custom-call(bf16[704,2048]{1,0:T(8,128)(2,1)} %bitcast.21, bf16[1,2048,512]{2,1,0:T(8,128)(2,1)} %gate_hbm.1, bf16[1,2048,512]{2,1,0:T(8,128)(2,1)} %up_hbm.1, bf16[1,512,2048]{2,1,0:T(8,128)(2,1)} %down_hbm.1, f32[8,128,88]{2,1,0:T(8,128)} %select_add_fusion.mix, ...), custom_call_target="tpu_custom_call" | custom-call | tf_op jit(solution)/shard_map/pallas_call | solution.py:540
  116.2 2.4 %copy.55 = bf16[256,2048]{1,0:T(8,128)(2,1)} copy(bf16[256,2048]{1,0:T(8,128)(2,1)} %get-tuple-element.34) | data formatting | bytes 2097152
  118.6 0.8 copy.56
  (34 shorter events, 0.9 us)
Async XLA Ops:
  0.6 10.5 %copy-start = (bf16[768,512]{1,0:T(8,128)(2,1)S(1)}, bf16[768,512]{1,0:T(8,128)(2,1)}, u32[]{:S(2)}) copy-start(bf16[768,512]{1,0:T(8,128)(2,1)} %param.22) | copy-start | bytes 2359300
  0.6 10.1 %copy-start.3 = (bf16[256,768]{1,0:T(8,128)(2,1)S(1)}, bf16[256,768]{1,0:T(8,128)(2,1)}, u32[]{:S(2)}) copy-start(bf16[256,768]{1,0:T(8,128)(2,1)} %param.17) | copy-start | bytes 1179652
  0.7 10.1 %copy-start.5 = (f32[768]{0:T(1024)S(1)}, f32[768]{0:T(1024)}, u32[]{:S(2)}) copy-start(f32[768]{0:T(1024)} %param.20) | copy-start | bytes 9220
  0.7 10.1 %copy-start.4 = (bf16[768,256]{1,0:T(8,128)(2,1)S(1)}, bf16[768,256]{1,0:T(8,128)(2,1)}, u32[]{:S(2)}) copy-start(bf16[768,256]{1,0:T(8,128)(2,1)} %param.23) | copy-start | bytes 1179652
  12.8 2.6 %copy-start.1 = (bf16[128,2048]{1,0:T(8,128)(2,1)S(1)}, bf16[128,2048]{1,0:T(8,128)(2,1)}, u32[]{:S(2)}) copy-start(bf16[128,2048]{1,0:T(8,128)(2,1)} %param.27) | copy-start | bytes 1572868
  116.2 2.4 %copy-start.2 = (bf16[128,2048]{1,0:T(8,128)(2,1)S(1)}, bf16[128,2048]{1,0:T(8,128)(2,1)}, u32[]{:S(2)}) copy-start(bf16[128,2048]{1,0:T(8,128)(2,1)} %get-tuple-element.35) | copy-start | bytes 1572868
where the time goes:
time: 120 us; the launch traced here: 119 us
  Pallas kernels  99.5 us (83%)
  other arithmetic  8.41 us (7%)
  local copies, waits for them, and re-layouts  8.35 us (7%)
  matrix products  2.29 us (2%)
    pallas_call x1, Pallas kernels, per_device(): pl.pallas_call(functools.partial(gather_kernel, n_ep, n_tp, heads), out_s...  50.2 us
    pallas_call x1, Pallas kernels, per_device(): pl.pallas_call(functools.partial(return_kernel, n_ep, n_tp), out_shape=(j...  49.3 us
    unnamed x16, local copies, waits for them, and re-layouts  4.07 us
    reduce_sum x3, other arithmetic, norm_scale(): jnp.mean(widened * widened, axis=-1, keepdims=True) + EPSILON  3.46 us

commit v1 on v0

--- a/solution.py
+++ b/solution.py
@@ -2,6 +2,7 @@
 
 import jax
 import jax.numpy as jnp
+import numpy as np
 from jax import lax
 from jax.experimental import pallas as pl
 from jax.experimental.pallas import tpu as pltpu
@@ -577,9 +578,584 @@
     return (mixer_output, expert_output)
 
 
+def take(src, dst, sem):
+    copy = pltpu.make_async_copy(src, dst, sem)
+    copy.start()
+    return copy
+
+
+def turn_pair(values, cosine, sine):
+    half = ROPE // 2
+    lane = lax.broadcasted_iota(jnp.int32, values.shape, 1)
+    upper = lax.rem(lane, ROPE) >= half
+    swapped = jnp.where(
+        upper, pltpu.roll(values, half, 1), -pltpu.roll(values, LANES - half, 1)
+    )
+    return values * cosine + swapped * sine
+
+
+def step_kernel(n_ep, n_tp, heads, *refs):
+    (
+        routing_h, share_h, ein_h, egain_h, slat_h, sgain_h, rkey_h, qlat_h, qgain_h, freq_h,
+        qp_h, qt_h, kw_h, vw_h, mw_h, gate_h, up_h, down_h,
+        eout, mout,
+        routing, share, ein, egain, slat, sgain, rkey, qlat, qgain, freq,
+        qp_w, qt_w, key_w, value_w, mixer_w, gate_w, up_w, down_w,
+        load_sem,
+        normed, ranks, weights, disp, arr, mixing,
+        lat_all, queries, keys, values, top, total, mixed, out,
+        part, ca, sums, ya, res, ret,
+        msend, mown, mca, msum, mya,
+        d_s, d_r, dy_s, dy_r, dc_s, dc_r,
+        lz_s, lz_r, lx_s, lx_r, lc_s, lc_r,
+        rc_s, rc_r, ry_s, ry_r, re_s, re_r,
+        mc_s, mc_r, my_s, my_r, mo_s, mo_r,
+        oy_s, oy_r, oc_s, oc_r,
+    ) = refs
+    me_e = lax.axis_index("ep")
+    me_t = lax.axis_index("tp")
+    depth = n_ep // 2
+    z = me_e // 2
+    x = lax.rem(me_e, 2)
+    y = me_t // CORES
+    c = lax.rem(me_t, CORES)
+    mate = y * CORES + (1 - c)
+    over = (1 - y) * CORES + c
+    far = (1 - y) * CORES + (1 - c)
+    tokens, width = ein.shape
+    capacity = arr.shape[1]
+    quarter = width // n_tp
+    half = width // CORES
+    rows = slat.shape[0]
+    rank = slat.shape[1]
+    head_keys = NOPE + LANES
+
+    loads = []
+    pairs = (
+        (routing_h, routing), (share_h, share), (ein_h, ein), (egain_h, egain),
+        (slat_h, slat), (sgain_h, sgain), (rkey_h, rkey), (freq_h, freq),
+        (qlat_h, qlat), (qgain_h, qgain), (qp_h, qp_w), (qt_h, qt_w),
+        (gate_h.at[0], gate_w), (up_h.at[0], up_w), (down_h.at[0], down_w),
+        (kw_h, key_w), (vw_h, value_w), (mw_h, mixer_w),
+    )
+    for n, (src, dst) in enumerate(pairs):
+        loads.append(take(src, dst, load_sem.at[n]))
+
+    def ready(first, last):
+        for n in range(first, last):
+            loads[n].wait()
+
+    def ep_at(d, f):
+        return lax.rem(z + d + depth, depth) * 2 + (x if f == 0 else 1 - x)
+
+    def cols(t):
+        return pl.ds(pl.multiple_of(t * quarter, LANES), quarter)
+
+    def side(core):
+        return pl.ds(pl.multiple_of(core * half, LANES), half)
+
+    barrier = pltpu.get_barrier_semaphore()
+    peers = [(ep_at(d, f), me_t) for d in range(depth) for f in range(2) if d or f]
+    peers += [(me_e, t) for t in (mate, over)]
+    for peer in peers:
+        pl.semaphore_signal(
+            barrier, inc=1, device_id=peer, device_id_type=pl.DeviceIdType.MESH
+        )
+
+    sends = []
+
+    def go(copy):
+        copy.start()
+        sends.append(copy)
+
+    ready(0, 2)
+    expert = lax.broadcasted_iota(jnp.int32, (n_ep, tokens), 0)
+    member = jnp.zeros((n_ep, tokens), F32)
+    weight = jnp.zeros((n_ep, tokens), F32)
+    for k in range(routing.shape[0]):
+        named = routing[k : k + 1, :] == expert
+        member = member + jnp.where(named, 1.0, 0.0)
+        weight = weight + jnp.where(named, share[k : k + 1, :], 0.0)
+    before = lax.broadcasted_iota(jnp.int32, (tokens, tokens), 0) < lax.broadcasted_iota(
+        jnp.int32, (tokens, tokens), 1
+    )
+    placed = jnp.dot(
+        member.astype(BF16),
+        jnp.where(before, 1.0, 0.0).astype(BF16),
+        preferred_element_type=F32,
+    )
+    placed = jnp.where(member > 0.0, placed, -1.0)
+    ranks[...] = placed
+    ready(2, 4)
+    normed[...] = norm_rows(ein[...], egain[...])
+    slot_row = lax.broadcasted_iota(jnp.int32, (capacity, tokens), 0).astype(F32)
+
+    def chosen(e):
+        return jnp.where(ranks[pl.ds(e, 1), :] == slot_row, 1.0, 0.0).astype(BF16)
+
+    own_cols = normed[:, cols(me_t)]
+    for d in range(depth):
+        for f in range(2):
+            if d or f:
+                disp[2 * d + f] = jnp.dot(
+                    chosen(ep_at(d, f)), own_cols, preferred_element_type=F32
+                ).astype(BF16)
+    pl.semaphore_wait(barrier, len(peers))
+
+    def disp_at(i, t):
+        return arr.at[i, :, cols(t)]
+
+    def direct(i):
+        return remote(
+            disp.at[i], disp_at(i, me_t), d_s.at[i], d_r.at[i], ep_at(i // 2, i % 2), me_t
+        )
+
+    for i in range(1, n_ep):
+        go(direct(i))
+
+    ready(4, 8)
+    position = lax.broadcasted_iota(jnp.int32, (rows, LANES), 0) + me_e * rows
+    angles = position.astype(F32) * freq[...]
+    cosine = jnp.cos(angles)
+    sine = jnp.sin(angles)
+    latent = norm_rows(slat[...], sgain[...])
+    lat_all[0, :, :rank] = latent
+    key_rows = rkey[...].astype(F32)
+    lat_all[0, :, rank:] = turn_pair(
+        jnp.concatenate([key_rows, key_rows], axis=1), cosine, sine
+    ).astype(BF16)
+    lat_rows = rows // CORES
+
+    def lat_at(i, core):
+        return lat_all.at[i, pl.ds(pl.multiple_of(core * lat_rows, lat_rows), lat_rows), :]
+
+    def lat_z(d):
+        return remote(
+            lat_at(0, c), lat_at(2 * d, c), lz_s.at[d], lz_r.at[d], ep_at(d, 0), me_t
+        )
+
+    def lat_x(d):
+        return remote(
+            lat_at(2 * d, c), lat_at(2 * d + 1, c), lx_s.at[d], lx_r.at[d], ep_at(0, 1), me_t
+        )
+
+    def lat_c(i, core):
+        return remote(lat_at(i, core), lat_at(i, core), lc_s.at[i], lc_r.at[i], me_e, mate)
+
+    go(lat_x(0))
+    for d in range(1, depth):
+        go(lat_z(d))
+
+    def z_arr(d):
+        lat_z(d).wait_recv()
+        go(lat_x(d))
+        go(lat_c(2 * d, c))
+
+    def x_arr(d):
+        lat_x(d).wait_recv()
+        go(lat_c(2 * d + 1, c))
+
+    arr[0] = jnp.dot(chosen(me_e), normed[...], preferred_element_type=F32).astype(BF16)
+    placed_t = jnp.transpose(placed)
+    weight_t = jnp.transpose(weight)
+    lane = lax.broadcasted_iota(jnp.int32, (tokens, n_ep), 1)
+    slot_col = lax.broadcasted_iota(jnp.int32, (tokens, capacity), 1).astype(F32)
+    for i in range(n_ep):
+        mine = lane == ep_at(i // 2, i % 2)
+        place = jnp.sum(jnp.where(mine, placed_t, 0.0), axis=1, keepdims=True)
+        scale = jnp.sum(jnp.where(mine, weight_t, 0.0), axis=1, keepdims=True)
+        mixing[i] = jnp.where(place == slot_col, scale, 0.0)
+
+    ready(8, 12)
+    query = norm_rows(qlat[...], qgain[...])
+    plain = jnp.dot(query, qp_w[...], preferred_element_type=F32).astype(BF16)
+    raw = jnp.dot(query, qt_w[...], preferred_element_type=F32)
+    group = lax.broadcasted_iota(jnp.int32, (rows, LANES), 1) // ROPE
+    for h in range(heads):
+        j = h * ROPE // LANES
+        turned = turn_pair(raw[:, j * LANES : (j + 1) * LANES], cosine, sine)
+        turned = jnp.where(group == h % (LANES // ROPE), turned, 0.0)
+        queries[:, h * head_keys : h * head_keys + NOPE] = plain[:, h * NOPE : (h + 1) * NOPE]
+        queries[:, h * head_keys + NOPE : (h + 1) * head_keys] = turned.astype(BF16)
+
+    def relay(i):
+        direct(i).wait_recv()
+        here = disp_at(i, me_t)
+        go(remote(here, here, dy_s.at[i], dy_r.at[i], me_e, over))
+        go(remote(here, here, dc_s.at[i, 0], dc_r.at[i, 0], me_e, mate))
+
+    def forward(i):
+        got = disp_at(i, over)
+        remote(got, got, dy_s.at[i], dy_r.at[i], me_e, over).wait_recv()
+        go(remote(got, got, dc_s.at[i, 1], dc_r.at[i, 1], me_e, mate))
+
+    def arrive(i):
+        for k, t in enumerate((mate, far)):
+            got = disp_at(i, t)
+            remote(got, got, dc_s.at[i, k], dc_r.at[i, k], me_e, mate).wait_recv()
+
+    def project(i):
+        at = slice(i * rows, (i + 1) * rows)
+        latent = lat_all[i, :, :rank]
+        k = jnp.dot(latent, key_w[...], preferred_element_type=F32).astype(BF16)
+        values[at, :] = jnp.dot(latent, value_w[...], preferred_element_type=F32).astype(BF16)
+        for h in range(heads):
+            keys[at, h * head_keys : h * head_keys + NOPE] = k[:, h * NOPE : (h + 1) * NOPE]
+            keys[at, h * head_keys + NOPE : (h + 1) * head_keys] = lat_all[i, :, rank:]
+
+    def core_copy(i, k):
+        t = mate if k == 0 else far
+        return remote(
+            part.at[i, :, cols(t)], ca.at[i, k], rc_s.at[i, k], rc_r.at[i, k], me_e, mate
+        )
+
+    def y_copy(i):
+        return remote(sums.at[i], ya.at[i], ry_s.at[i], ry_r.at[i], me_e, over)
+
+    def back(i):
+        return remote(res.at[i], ret.at[i], re_s.at[i], re_r.at[i], ep_at(-(i // 2), i % 2), me_t)
+
+    def y_step(i):
+        core_copy(i, 1).wait_recv()
+        sums[i] = (ca[i, 1].astype(F32) + part[i, :, cols(over)].astype(F32)).astype(BF16)
+        go(y_copy(i))
+
+    def sum_step(i):
+        core_copy(i, 0).wait_recv()
+        value = ca[i, 0].astype(F32) + part[i, :, cols(me_t)].astype(F32)
+        y_copy(i).wait_recv()
+        value = (value + ya[i].astype(F32)).astype(BF16)
+        if i == 0:
+            ret[0] = value
+        else:
+            res[i] = value
+            go(back(i))
+
+    def chunk(d, between):
+        rows_in = arr[2 * d : 2 * d + 2].reshape(2 * capacity, width)
+        gate = jnp.minimum(jnp.dot(rows_in, gate_w[...], preferred_element_type=F32), CLAMP_LIMIT)
+        between()
+        up = jnp.clip(
+            jnp.dot(rows_in, up_w[...], preferred_element_type=F32), -CLAMP_LIMIT, CLAMP_LIMIT
+        )
+        hidden = ((up + 1.0) * (gate * jax.nn.sigmoid(SLOPE * gate))).astype(BF16)
+        value = jnp.dot(hidden, down_w[...], preferred_element_type=F32)
+        part[2 * d] = value[:capacity].astype(BF16)
+        part[2 * d + 1] = value[capacity:].astype(BF16)
+        for i in (2 * d, 2 * d + 1):
+            for k in (1, 0):
+                go(core_copy(i, k))
+
+    log2e = 1.4426950408889634
+    scaling = (NOPE + ROPE) ** (-0.5) * log2e
+
+    def attend(h, first, last):
+        at = slice(first * rows, last * rows)
+        head = slice(h * head_keys, (h + 1) * head_keys)
+        scores = lax.dot_general(
+            queries[:, head], keys[at, head], (((1,), (1,)), ((), ())), preferred_element_type=F32
+        )
+        pieces = []
+        for i in range(first, last):
+            piece = scores[:, (i - first) * rows : (i - first + 1) * rows]
+            if i == 0:
+                row = lax.broadcasted_iota(jnp.int32, (rows, rows), 0)
+                piece = jnp.where(
+                    lax.broadcasted_iota(jnp.int32, (rows, rows), 1) <= row, piece, NEGATIVE
+                )
+            else:
+                piece = piece + jnp.where(ep_at(-(i // 2), i % 2) < me_e, 0.0, NEGATIVE)
+            pieces.append(piece)
+        scores = jnp.concatenate(pieces, axis=1)
+        peak = jnp.max(scores, axis=-1, keepdims=True)
+        if first > 0:
+            old = top[h]
+            peak = jnp.maximum(peak, old)
+        weight = jnp.exp2((scores - peak) * scaling)
+        sum_of = jnp.sum(weight, axis=-1, keepdims=True)
+        term = jnp.dot(
+            weight.astype(BF16), values[at, h * VDIM : (h + 1) * VDIM], preferred_element_type=F32
+        )
+        if first > 0:
+            fade = jnp.exp2((old - peak) * scaling)
+            sum_of = sum_of + fade * total[h]
+            term = term + fade * mixed[h]
+        if last < n_ep:
+            top[h] = peak
+            total[h] = sum_of
+            mixed[h] = term
+        else:
+            out[:, h * VDIM : (h + 1) * VDIM] = (term / sum_of).astype(BF16)
+
+    def lat_arrive(i):
+        lat_c(i, 1 - c).wait_recv()
+
+    acc = []
+
+    def mix(i):
+        if i > 0:
+            back(i).wait_recv()
+        table = mixing[i]
+        high = table.astype(BF16)
+        low = (table - high.astype(F32)).astype(BF16)
+        term = jnp.dot(high, ret[i], preferred_element_type=F32) + jnp.dot(
+            low, ret[i], preferred_element_type=F32
+        )
+        acc[:] = [term if not acc else acc[0] + term]
+
+    def out_copy(k, t, to):
+        ref = eout.at[:, cols(t)]
+        s, r = (oy_s, oy_r) if k == 0 else (oc_s, oc_r)
+        n = 0 if k < 2 else 1
+        return remote(ref, ref, s.at[n], r.at[n], me_e, to)
+
+    def mix_rows(n):
+        return slice(n * lat_rows, (n + 1) * lat_rows)
+
+    def mixer_core(n):
+        return remote(
+            msend.at[mix_rows(n)], mca.at[mix_rows(n)], mc_s.at[n], mc_r.at[n], me_e, mate
+        )
+
+    def mixer_y(n):
+        return remote(
+            msum.at[mix_rows(n)], mya.at[mix_rows(n)], my_s.at[n], my_r.at[n], me_e, over
+        )
+
+    def mixer_out(n, core):
+        ref = mout.at[mix_rows(n), side(core)]
+        return remote(ref, ref, mo_s.at[n], mo_r.at[n], me_e, mate)
+
+    ready(15, 17)
+    project(0)
+    relay(1)
+    relay(2)
+    forward(1)
+    relay(3)
+    forward(2)
+    arrive(1)
+    ready(12, 15)
+    for d in range(depth):
+
+        def between(d=d):
+            if d + 2 < depth:
+                relay(2 * d + 4)
+                forward(2 * d + 3)
+                relay(2 * d + 5)
+                forward(2 * d + 4)
+            elif d + 2 == depth:
+                forward(2 * d + 3)
+                x_arr(0)
+            else:
+                z_arr(1)
+
+        chunk(d, between)
+        if d > 0:
+            for i in (2 * d - 2, 2 * d - 1):
+                y_step(i)
+        if d > 1:
+            for i in (2 * d - 4, 2 * d - 3):
+                sum_step(i)
+        if d + 1 < depth:
+            for i in (2 * d + 2, 2 * d + 3):
+                arrive(i)
+    lat_arrive(1)
+    project(1)
+    y_step(n_ep - 2)
+    y_step(n_ep - 1)
+    x_arr(1)
+    lat_arrive(2)
+    project(2)
+    for d in range(2, depth):
+        z_arr(d)
+    sum_step(n_ep - 4)
+    sum_step(n_ep - 3)
+    lat_arrive(3)
+    project(3)
+    middle = n_ep // 2
+    attend(0, 0, middle)
+    sum_step(n_ep - 2)
+    sum_step(n_ep - 1)
+    for d in range(2, depth):
+        x_arr(d)
+    for h in range(1, heads):
+        attend(h, 0, middle)
+    for i in range(middle, n_ep):
+        lat_arrive(i)
+        project(i)
+    todo = list(range(n_ep))
+    for h in range(heads):
+        attend(h, middle, n_ep)
+        for i in todo[h * n_ep // heads : (h + 1) * n_ep // heads]:
+            mix(i)
+    eout[:, cols(me_t)] = acc[0].astype(BF16)
+    go(out_copy(0, me_t, over))
+    go(out_copy(1, me_t, mate))
+    ready(17, 18)
+    msend[...] = jnp.dot(
+        out[...], mixer_w[:, side(1 - c)], preferred_element_type=F32
+    ).astype(BF16)
+    for n in range(2):
+        go(mixer_core(n))
+    mown[...] = jnp.dot(out[...], mixer_w[:, side(c)], preferred_element_type=F32)
+    for n in range(2):
+        mixer_core(n).wait_recv()
+        at = mix_rows(n)
+        msum[at] = (mown[at] + mca[at].astype(F32)).astype(BF16)
+        go(mixer_y(n))
+    out_copy(0, over, over).wait_recv()
+    go(out_copy(2, over, mate))
+    for n in range(2):
+        mixer_y(n).wait_recv()
+        at = mix_rows(n)
+        mout[at, side(c)] = (msum[at].astype(F32) + mya[at].astype(F32)).astype(BF16)
+        go(mixer_out(n, c))
+    out_copy(1, mate, mate).wait_recv()
+    out_copy(2, far, mate).wait_recv()
+    for n in range(2):
+        mixer_out(n, 1 - c).wait_recv()
+    for copy in sends:
+        copy.wait_send()
+
+
+def fused(
+    n_ep,
+    n_tp,
+    query_latent,
+    shared_latent,
+    rotary_key,
+    query_gain,
+    shared_gain,
+    query_plain_weight,
+    query_turn_weight,
+    key_weight,
+    value_weight,
+    mixer_out_weight,
+    expert_input,
+    expert_gain,
+    routing,
+    routing_weight,
+    gate_weight,
+    up_weight,
+    down_weight,
+):
+    rows, query_rank = query_latent.shape
+    rank = shared_latent.shape[1]
+    heads = query_plain_weight.shape[1] // NOPE
+    tokens, width = expert_input.shape
+    top_count = routing.shape[1]
+    units = gate_weight.shape[2]
+    capacity = 4 * tokens * top_count // (3 * n_ep)
+    capacity = -(-capacity // 8) * 8
+    quarter = width // n_tp
+    half = width // CORES
+    depth = n_ep // 2
+    total = n_ep * rows
+    lane = np.arange(LANES)
+    freq = ROTARY_BASE ** (-2.0 * (lane % (ROPE // 2)) / ROPE)
+    freq = jnp.asarray(freq.astype(np.float32)[None, :])
+    args = (
+        routing.T,
+        routing_weight.T,
+        expert_input,
+        expert_gain[None, :],
+        shared_latent,
+        shared_gain[None, :],
+        rotary_key,
+        query_latent,
+        query_gain[None, :],
+        freq,
+        query_plain_weight,
+        query_turn_weight,
+        key_weight,
+        value_weight,
+        mixer_out_weight,
+        gate_weight,
+        up_weight,
+        down_weight,
+    )
+    dma = pltpu.SemaphoreType.DMA
+    held = [pltpu.VMEM(a.shape if a.ndim == 2 else a.shape[1:], a.dtype) for a in args]
+    expert_output, mixer_output = pl.pallas_call(
+        functools.partial(step_kernel, n_ep, n_tp, heads),
+        out_shape=(
+            jax.ShapeDtypeStruct((tokens, width), BF16),
+            jax.ShapeDtypeStruct((rows, width), BF16),
+        ),
+        in_specs=[pl.BlockSpec(memory_space=pl.ANY)] * len(args),
+        out_specs=vmem(2),
+        scratch_shapes=held
+        + [
+            dma((len(args),)),
+            pltpu.VMEM((tokens, width), BF16),
+            pltpu.VMEM((n_ep, tokens), F32),
+            pltpu.VMEM((n_ep, tokens), F32),
+            pltpu.VMEM((n_ep, capacity, quarter), BF16),
+            pltpu.VMEM((n_ep, capacity, width), BF16),
+            pltpu.VMEM((n_ep, tokens, capacity), F32),
+            pltpu.VMEM((n_ep, rows, rank + LANES), BF16),
+            pltpu.VMEM((rows, heads * (NOPE + LANES)), BF16),
+            pltpu.VMEM((total, heads * (NOPE + LANES)), BF16),
+            pltpu.VMEM((total, heads * VDIM), BF16),
+            pltpu.VMEM((heads, rows, 1), F32),
+            pltpu.VMEM((heads, rows, 1), F32),
+            pltpu.VMEM((heads, rows, VDIM), F32),
+            pltpu.VMEM((rows, heads * VDIM), BF16),
+            pltpu.VMEM((n_ep, capacity, width), BF16),
+            pltpu.VMEM((n_ep, CORES, capacity, quarter), BF16),
+            pltpu.VMEM((n_ep, capacity, quarter), BF16),
+            pltpu.VMEM((n_ep, capacity, quarter), BF16),
+            pltpu.VMEM((n_ep, capacity, quarter), BF16),
+            pltpu.VMEM((n_ep, capacity, quarter), BF16),
+            pltpu.VMEM((rows, half), BF16),
+            pltpu.VMEM((rows, half), F32),
+            pltpu.VMEM((rows, half), BF16),
+            pltpu.VMEM((rows, half), BF16),
+            pltpu.VMEM((rows, half), BF16),
+            dma((n_ep,)),
+            dma((n_ep,)),
+            dma((n_ep,)),
+            dma((n_ep,)),
+            dma((n_ep, 2)),
+            dma((n_ep, 2)),
+            dma((depth,)),
+            dma((depth,)),
+            dma((depth,)),
+            dma((depth,)),
+            dma((n_ep,)),
+            dma((n_ep,)),
+            dma((n_ep, 2)),
+            dma((n_ep, 2)),
+            dma((n_ep,)),
+            dma((n_ep,)),
+            dma((n_ep,)),
+            dma((n_ep,)),
+            dma((2,)),
+            dma((2,)),
+            dma((2,)),
+            dma((2,)),
+            dma((2,)),
+            dma((2,)),
+            dma((1,)),
+            dma((1,)),
+            dma((2,)),
+            dma((2,)),
+        ],
+        compiler_params=pltpu.CompilerParams(
+            collective_id=2, has_side_effects=True, vmem_limit_bytes=VMEM_LIMIT
+        ),
+    )(*args)
+    return (mixer_output, expert_output)
+
+
+def pick(mesh):
+    small = mesh.shape["tp"] == 2 * CORES and mesh.shape["ep"] <= 8 and mesh.shape["ep"] % 4 == 0
+    return fused if small else per_device
+
+
 def solution(mesh):
     return jax.shard_map(
-        functools.partial(per_device, mesh.shape["ep"], mesh.shape["tp"]),
+        functools.partial(pick(mesh), mesh.shape["ep"], mesh.shape["tp"]),
         mesh=mesh,
         in_specs=(
             P("ep", None),

time: 120 us -> 93.1 us (0.78)
  Pallas kernels: 99.5 us -> 85 us
  other arithmetic: 8.41 us -> 0 us
  local copies, waits for them, and re-layouts: 8.35 us -> 5.92 us
  matrix products: 2.29 us -> 0 us
    pallas_call x2 -> x1, Pallas kernels: 99.5 us -> 85 us  [fused(): pl.pallas_call(functools.partial(step_kernel, n_ep, n_tp, heads), out_sha...]
    reduce_sum x3 -> x0, other arithmetic: 3.46 us -> none  [norm_scale(): jnp.mean(widened * widened, axis=-1, keepdims=True) + EPSILON]
    convert_element_type x6 -> x0, other arithmetic: 2.47 us -> none  [the longest x1 1.22 us: per_device(): query_turned = rotate_heads(query_raw, position).astype(BF16)]
    dot_general x4 -> x0, matrix products: 2.29 us -> none  [the longest x1 1.28 us: per_device(): jnp.dot(table.astype(BF16), normed, preferred_element_type=F32).astype(BF16)]
    add x2 -> x0, other arithmetic: 1.77 us -> none  [the longest x1 1.07 us: per_device(): mixing + jnp.where(target[:, k][:, None] == slot_ids[None, :], routing_we...]
    dynamic_slice x2 -> x0, local copies, waits for them, and re-layouts: 1.55 us -> none  [the longest x1 0.79 us: per_device(): lax.dynamic_slice_in_dim(rotary_key, first, share, 0).astype(F32)]
    unnamed x16 -> x5, local copies, waits for them, and re-layouts: 4.07 us -> 4.65 us
where the time goes in v1:
time: 93.1 us; the launch traced here: 91.5 us
  Pallas kernels  85 us (91%)
  local copies, waits for them, and re-layouts  5.92 us (6%)
    pallas_call x1, Pallas kernels, fused(): pl.pallas_call(functools.partial(step_kernel, n_ep, n_tp, heads), out_sha...  85 us
    unnamed x5, local copies, waits for them, and re-layouts  4.65 us

profile of v1, /device:TPU:0, one launch (start us, length us, event | category | flops | bytes accessed | tf_op | source)
XLA Modules:
  0.0 91.5 jit_solution(5507553412236413140)
XLA Ops:
  0.6 1.3 %broadcast_in_dim.11.refs_8_ = f32[1,768]{1,0:T(1,128)} reshape(f32[768]{0:T(1024)} %param.21) | data formatting | bytes 6144 | tf_op jit(solution)/shard_map/broadcast_in_dim | solution.py:1066
  1.9 1.5 %copy.20.refs_6_ = bf16[256,64]{1,0:T(8,128)(2,1)} copy(bf16[256,64]{0,1:T(8,128)(2,1)} %param.20) | data formatting | bytes 65536 | tf_op args[2]
  3.4 85.0 %shard_map.185 = (bf16[128,2048]{1,0:T(8,128)(2,1)}, bf16[256,2048]{1,0:T(8,128)(2,1)}) custom-call(s32[4,128]{1,0:T(4,128)} %bitcast.5, f32[4,128]{1,0:T(4,128)} %bitcast.6, bf16[128,2048]{1,0:T(8,128)(2,1)} %refs_2_.1, f32[1,2048]{1,0:T(1,128)} %bitcast.4, bf16[256,512]{1,0:T(8,128)(2,1)} %refs_4_.1, f32[1,512]{1,0:T(1,128)} %bitcast.7, ...), custom_call_target="tpu_custom_call" | custom-call | tf_op jit(solution)/shard_map/pallas_call | solution.py:1079
  88.4 0.0 copy-start
  88.4 2.4 %copy.23 = bf16[256,2048]{1,0:T(8,128)(2,1)} copy(bf16[256,2048]{1,0:T(8,128)(2,1)} %get-tuple-element.8) | data formatting | bytes 2097152
  90.7 0.0 copy-done
  90.7 0.8 copy.24
Async XLA Ops:
  88.4 2.4 %copy-start = (bf16[128,2048]{1,0:T(8,128)(2,1)S(1)}, bf16[128,2048]{1,0:T(8,128)(2,1)}, u32[]{:S(2)}) copy-start(bf16[128,2048]{1,0:T(8,128)(2,1)} %get-tuple-element.9) | copy-start | bytes 1572868

commit v2 on v1

--- a/solution.py
+++ b/solution.py
@@ -20,6 +20,7 @@
 ROTARY_BASE = 10000.0
 NEGATIVE = -1e30
 VMEM_LIMIT = 60 * 1024 * 1024
+FUSED_LIMIT = 58 * 1024 * 1024
 F32 = jnp.float32
 BF16 = jnp.bfloat16
 
@@ -654,6 +655,7 @@
     def side(core):
         return pl.ds(pl.multiple_of(core * half, LANES), half)
 
+    lat_all[1:] = jnp.zeros((n_ep - 1, rows, rank + LANES), BF16)
     barrier = pltpu.get_barrier_semaphore()
     peers = [(ep_at(d, f), me_t) for d in range(depth) for f in range(2) if d or f]
     peers += [(me_e, t) for t in (mate, over)]
@@ -664,9 +666,15 @@
 
     sends = []
 
-    def go(copy):
-        copy.start()
-        sends.append(copy)
+    def go(copy, when=None):
+        if when is None:
+            copy.start()
+        else:
+            pl.when(when)(copy.start)
+        sends.append((when, copy))
+
+    def landed(copy, when):
+        pl.when(when)(copy.wait_recv)
 
     ready(0, 2)
     expert = lax.broadcasted_iota(jnp.int32, (n_ep, tokens), 0)
@@ -687,7 +695,7 @@
     placed = jnp.where(member > 0.0, placed, -1.0)
     ranks[...] = placed
     ready(2, 4)
-    normed[...] = norm_rows(ein[...], egain[...])
+    normed[...] = norm_rows(ein[...], egain[...][None, :])
     slot_row = lax.broadcasted_iota(jnp.int32, (capacity, tokens), 0).astype(F32)
 
     def chosen(e):
@@ -710,17 +718,19 @@
             disp.at[i], disp_at(i, me_t), d_s.at[i], d_r.at[i], ep_at(i // 2, i % 2), me_t
         )
 
-    for i in range(1, n_ep):
-        go(direct(i))
+    spread = [1, depth - 1] + list(range(2, depth - 1))
+    go(direct(1))
+    for f in range(2):
+        go(direct(2 * spread[0] + f))
 
     ready(4, 8)
     position = lax.broadcasted_iota(jnp.int32, (rows, LANES), 0) + me_e * rows
     angles = position.astype(F32) * freq[...]
     cosine = jnp.cos(angles)
     sine = jnp.sin(angles)
-    latent = norm_rows(slat[...], sgain[...])
+    latent = norm_rows(slat[...], sgain[...][None, :])
     lat_all[0, :, :rank] = latent
-    key_rows = rkey[...].astype(F32)
+    key_rows = jnp.transpose(rkey[...].astype(F32))
     lat_all[0, :, rank:] = turn_pair(
         jnp.concatenate([key_rows, key_rows], axis=1), cosine, sine
     ).astype(BF16)
@@ -731,7 +741,7 @@
 
     def lat_z(d):
         return remote(
-            lat_at(0, c), lat_at(2 * d, c), lz_s.at[d], lz_r.at[d], ep_at(d, 0), me_t
+            lat_at(2 * d - 2, c), lat_at(2 * d, c), lz_s.at[d], lz_r.at[d], ep_at(1, 0), me_t
         )
 
     def lat_x(d):
@@ -742,18 +752,28 @@
     def lat_c(i, core):
         return remote(lat_at(i, core), lat_at(i, core), lc_s.at[i], lc_r.at[i], me_e, mate)
 
-    go(lat_x(0))
-    for d in range(1, depth):
-        go(lat_z(d))
+    def lat_up(d):
+        if d + 1 < depth:
+            go(lat_z(d + 1), jnp.logical_and(z >= d, z < depth - 1))
+
+    def known(i):
+        return x == 1 if i == 1 else z >= i // 2
+
+    go(lat_x(0), x == 0)
+    lat_up(0)
+    for d in spread[1:]:
+        for f in range(2):
+            go(direct(2 * d + f))
 
     def z_arr(d):
-        lat_z(d).wait_recv()
-        go(lat_x(d))
-        go(lat_c(2 * d, c))
+        landed(lat_z(d), known(2 * d))
+        lat_up(d)
+        go(lat_x(d), known(2 * d))
+        go(lat_c(2 * d, c), known(2 * d))
 
     def x_arr(d):
-        lat_x(d).wait_recv()
-        go(lat_c(2 * d + 1, c))
+        landed(lat_x(d), known(2 * d + 1))
+        go(lat_c(2 * d + 1, c), known(2 * d + 1))
 
     arr[0] = jnp.dot(chosen(me_e), normed[...], preferred_element_type=F32).astype(BF16)
     placed_t = jnp.transpose(placed)
@@ -767,7 +787,7 @@
         mixing[i] = jnp.where(place == slot_col, scale, 0.0)
 
     ready(8, 12)
-    query = norm_rows(qlat[...], qgain[...])
+    query = norm_rows(qlat[...], qgain[...][None, :])
     plain = jnp.dot(query, qp_w[...], preferred_element_type=F32).astype(BF16)
     raw = jnp.dot(query, qt_w[...], preferred_element_type=F32)
     group = lax.broadcasted_iota(jnp.int32, (rows, LANES), 1) // ROPE
@@ -831,10 +851,9 @@
             res[i] = value
             go(back(i))
 
-    def chunk(d, between):
+    def chunk(d):
         rows_in = arr[2 * d : 2 * d + 2].reshape(2 * capacity, width)
         gate = jnp.minimum(jnp.dot(rows_in, gate_w[...], preferred_element_type=F32), CLAMP_LIMIT)
-        between()
         up = jnp.clip(
             jnp.dot(rows_in, up_w[...], preferred_element_type=F32), -CLAMP_LIMIT, CLAMP_LIMIT
         )
@@ -888,7 +907,7 @@
             out[:, h * VDIM : (h + 1) * VDIM] = (term / sum_of).astype(BF16)
 
     def lat_arrive(i):
-        lat_c(i, 1 - c).wait_recv()
+        landed(lat_c(i, 1 - c), known(i))
 
     acc = []
 
@@ -909,8 +928,11 @@
         n = 0 if k < 2 else 1
         return remote(ref, ref, s.at[n], r.at[n], me_e, to)
 
+    pieces = 4
+    step = rows // pieces
+
     def mix_rows(n):
-        return slice(n * lat_rows, (n + 1) * lat_rows)
+        return slice(n * step, (n + 1) * step)
 
     def mixer_core(n):
         return remote(
@@ -926,96 +948,107 @@
         ref = mout.at[mix_rows(n), side(core)]
         return remote(ref, ref, mo_s.at[n], mo_r.at[n], me_e, mate)
 
+    first, second, third = (2 * d for d in spread)
+    middle = n_ep // 2
     ready(15, 17)
     project(0)
     relay(1)
-    relay(2)
+    relay(first)
+    relay(first + 1)
     forward(1)
-    relay(3)
-    forward(2)
+    x_arr(0)
+    z_arr(1)
     arrive(1)
     ready(12, 15)
-    for d in range(depth):
-
-        def between(d=d):
-            if d + 2 < depth:
-                relay(2 * d + 4)
-                forward(2 * d + 3)
-                relay(2 * d + 5)
-                forward(2 * d + 4)
-            elif d + 2 == depth:
-                forward(2 * d + 3)
-                x_arr(0)
-            else:
-                z_arr(1)
-
-        chunk(d, between)
-        if d > 0:
-            for i in (2 * d - 2, 2 * d - 1):
-                y_step(i)
-        if d > 1:
-            for i in (2 * d - 4, 2 * d - 3):
-                sum_step(i)
-        if d + 1 < depth:
-            for i in (2 * d + 2, 2 * d + 3):
-                arrive(i)
+    chunk(0)
+    forward(first)
+    forward(first + 1)
+    relay(second)
+    relay(second + 1)
+    y_step(0)
+    y_step(1)
+    z_arr(2)
+    x_arr(1)
+    arrive(first)
+    arrive(first + 1)
+    chunk(first // 2)
     lat_arrive(1)
     project(1)
-    y_step(n_ep - 2)
-    y_step(n_ep - 1)
-    x_arr(1)
-    lat_arrive(2)
-    project(2)
-    for d in range(2, depth):
-        z_arr(d)
-    sum_step(n_ep - 4)
-    sum_step(n_ep - 3)
-    lat_arrive(3)
-    project(3)
-    middle = n_ep // 2
-    attend(0, 0, middle)
-    sum_step(n_ep - 2)
-    sum_step(n_ep - 1)
-    for d in range(2, depth):
-        x_arr(d)
-    for h in range(1, heads):
+    forward(second)
+    forward(second + 1)
+    relay(third)
+    relay(third + 1)
+    z_arr(3)
+    x_arr(2)
+    y_step(first)
+    y_step(first + 1)
+    sum_step(0)
+    sum_step(1)
+    arrive(second)
+    arrive(second + 1)
+    chunk(second // 2)
+    for i in range(2, middle):
+        lat_arrive(i)
+        project(i)
+    forward(third)
+    forward(third + 1)
+    x_arr(3)
+    y_step(second)
+    y_step(second + 1)
+    sum_step(first)
+    sum_step(first + 1)
+    for h in range(heads // 2):
         attend(h, 0, middle)
+    arrive(third)
+    arrive(third + 1)
+    chunk(third // 2)
+    for h in range(heads // 2, heads):
+        attend(h, 0, middle)
+    y_step(third)
+    y_step(third + 1)
     for i in range(middle, n_ep):
         lat_arrive(i)
         project(i)
-    todo = list(range(n_ep))
+    sum_step(second)
+    sum_step(second + 1)
     for h in range(heads):
         attend(h, middle, n_ep)
-        for i in todo[h * n_ep // heads : (h + 1) * n_ep // heads]:
-            mix(i)
-    eout[:, cols(me_t)] = acc[0].astype(BF16)
-    go(out_copy(0, me_t, over))
-    go(out_copy(1, me_t, mate))
     ready(17, 18)
     msend[...] = jnp.dot(
         out[...], mixer_w[:, side(1 - c)], preferred_element_type=F32
     ).astype(BF16)
-    for n in range(2):
+    for n in range(pieces):
         go(mixer_core(n))
     mown[...] = jnp.dot(out[...], mixer_w[:, side(c)], preferred_element_type=F32)
-    for n in range(2):
+    sum_step(third)
+    sum_step(third + 1)
+    for n in range(pieces):
         mixer_core(n).wait_recv()
         at = mix_rows(n)
         msum[at] = (mown[at] + mca[at].astype(F32)).astype(BF16)
         go(mixer_y(n))
-    out_copy(0, over, over).wait_recv()
-    go(out_copy(2, over, mate))
-    for n in range(2):
+    for i in (0, first, second, third):
+        mix(i)
+        mix(i + 1)
+    eout[:, cols(me_t)] = acc[0].astype(BF16)
+    go(out_copy(0, me_t, over))
+    go(out_copy(1, me_t, mate))
+    for n in range(pieces):
         mixer_y(n).wait_recv()
         at = mix_rows(n)
         mout[at, side(c)] = (msum[at].astype(F32) + mya[at].astype(F32)).astype(BF16)
         go(mixer_out(n, c))
+    out_copy(0, over, over).wait_recv()
+    go(out_copy(2, over, mate))
     out_copy(1, mate, mate).wait_recv()
     out_copy(2, far, mate).wait_recv()
-    for n in range(2):
+    for n in range(pieces):
         mixer_out(n, 1 - c).wait_recv()
-    for copy in sends:
-        copy.wait_send()
+    for when, copy in sends:
+        if when is None:
+            copy.wait_send()
+        else:
+            pl.when(when)(copy.wait_send)
 
 
 def fused(
@@ -1058,12 +1091,12 @@
         routing.T,
         routing_weight.T,
         expert_input,
-        expert_gain[None, :],
+        expert_gain,
         shared_latent,
-        shared_gain[None, :],
-        rotary_key,
+        shared_gain,
+        rotary_key.T,
         query_latent,
-        query_gain[None, :],
+        query_gain,
         freq,
         query_plain_weight,
         query_turn_weight,
@@ -1075,14 +1108,14 @@
         down_weight,
     )
     dma = pltpu.SemaphoreType.DMA
-    held = [pltpu.VMEM(a.shape if a.ndim == 2 else a.shape[1:], a.dtype) for a in args]
+    held = [pltpu.VMEM(a.shape[1:] if a.ndim == 3 else a.shape, a.dtype) for a in args]
     expert_output, mixer_output = pl.pallas_call(
         functools.partial(step_kernel, n_ep, n_tp, heads),
         out_shape=(
             jax.ShapeDtypeStruct((tokens, width), BF16),
             jax.ShapeDtypeStruct((rows, width), BF16),
         ),
-        in_specs=[pl.BlockSpec(memory_space=pl.ANY)] * len(args),
+        in_specs=[pl.BlockSpec(memory_space=pltpu.HBM)] * len(args),
         out_specs=vmem(2),
         scratch_shapes=held
         + [
@@ -1130,26 +1163,26 @@
             dma((n_ep,)),
             dma((n_ep,)),
             dma((n_ep,)),
-            dma((2,)),
-            dma((2,)),
-            dma((2,)),
-            dma((2,)),
-            dma((2,)),
-            dma((2,)),
+            dma((4,)),
+            dma((4,)),
+            dma((4,)),
+            dma((4,)),
+            dma((4,)),
+            dma((4,)),
             dma((1,)),
             dma((1,)),
             dma((2,)),
             dma((2,)),
         ],
         compiler_params=pltpu.CompilerParams(
-            collective_id=2, has_side_effects=True, vmem_limit_bytes=VMEM_LIMIT
+            collective_id=2, has_side_effects=True, vmem_limit_bytes=FUSED_LIMIT
         ),
     )(*args)
     return (mixer_output, expert_output)
 
 
 def pick(mesh):
-    small = mesh.shape["tp"] == 2 * CORES and mesh.shape["ep"] <= 8 and mesh.shape["ep"] % 4 == 0
+    small = mesh.shape["tp"] == 2 * CORES and mesh.shape["ep"] == 8
     return fused if small else per_device
 
 

time: 93.1 us -> 76 us (0.82); the launches traced: 91.5 us -> 75.8 us
  Pallas kernels: 85 us -> 72 us
  local copies, waits for them, and re-layouts: 5.92 us -> 3.16 us
    pallas_call x1, Pallas kernels: 85 us -> 72 us  [fused(): pl.pallas_call(functools.partial(step_kernel, n_ep, n_tp, heads), out_sha...]
    unnamed x5 -> x4, local copies, waits for them, and re-layouts: 4.65 us -> 3.16 us
    broadcast_in_dim x1 -> x0, local copies, waits for them, and re-layouts: 1.27 us -> none  [fused(): query_gain[None, :]]
where the time goes in v2:
time: 76 us; the launch traced here: 75.8 us
  Pallas kernels  72 us (95%)
  local copies, waits for them, and re-layouts  3.16 us (4%)
    pallas_call x1, Pallas kernels, fused(): pl.pallas_call(functools.partial(step_kernel, n_ep, n_tp, heads), out_sha...  72 us
    unnamed x4, local copies, waits for them, and re-layouts  3.16 us

profile of v2, /device:TPU:0, one launch (start us, length us, event | category | flops | bytes accessed | tf_op | source)
XLA Modules:
  0.0 75.8 jit_solution(1184742875415351161)
XLA Ops:
  0.6 72.0 %shard_map.185 = (bf16[128,2048]{1,0:T(8,128)(2,1)}, bf16[256,2048]{1,0:T(8,128)(2,1)}) custom-call(s32[4,128]{1,0:T(4,128)} %bitcast.4, f32[4,128]{1,0:T(4,128)} %bitcast.5, bf16[128,2048]{1,0:T(8,128)(2,1)} %refs_2_.1, f32[2048]{0:T(1024)} %refs_3_.1, bf16[256,512]{1,0:T(8,128)(2,1)} %refs_4_.1, f32[512]{0:T(512)} %refs_5_.1, bf16[64,256]{1,0:T(8,128)(2,1)} %bitcast.3, ...), custom_call_target="tpu_custom_call" | custom-call | tf_op jit(solution)/shard_map/pallas_call | solution.py:1112
  72.6 0.0 copy-start
  72.7 2.4 %copy.22 = bf16[256,2048]{1,0:T(8,128)(2,1)} copy(bf16[256,2048]{1,0:T(8,128)(2,1)} %get-tuple-element.8) | data formatting | bytes 2097152
  75.0 0.0 copy-done
  75.0 0.8 %copy.23 = bf16[128,2048]{1,0:T(8,128)(2,1)} copy(bf16[128,2048]{1,0:T(8,128)(2,1)S(1)} %copy-done) | data formatting | bytes 1048576
Async XLA Ops:
  72.6 2.4 %copy-start = (bf16[128,2048]{1,0:T(8,128)(2,1)S(1)}, bf16[128,2048]{1,0:T(8,128)(2,1)}, u32[]{:S(2)}) copy-start(bf16[128,2048]{1,0:T(8,128)(2,1)} %get-tuple-element.9) | copy-start | bytes 1572868

commit v3 on v2

--- a/solution.py
+++ b/solution.py
@@ -20,6 +20,7 @@
 ROTARY_BASE = 10000.0
 NEGATIVE = -1e30
 VMEM_LIMIT = 60 * 1024 * 1024
+PARTS = 4
 FUSED_LIMIT = 58 * 1024 * 1024
 F32 = jnp.float32
 BF16 = jnp.bfloat16
@@ -599,7 +600,8 @@
     (
         routing_h, share_h, ein_h, egain_h, slat_h, sgain_h, rkey_h, qlat_h, qgain_h, freq_h,
         qp_h, qt_h, kw_h, vw_h, mw_h, gate_h, up_h, down_h,
-        eout, mout,
+        eout_h, mout_h,
+        eout, mout, keep_sem,
         routing, share, ein, egain, slat, sgain, rkey, qlat, qgain, freq,
         qp_w, qt_w, key_w, value_w, mixer_w, gate_w, up_w, down_w,
         load_sem,
@@ -633,8 +635,8 @@
 
     loads = []
     pairs = (
+        (slat_h, slat), (sgain_h, sgain), (rkey_h, rkey), (freq_h, freq),
         (routing_h, routing), (share_h, share), (ein_h, ein), (egain_h, egain),
-        (slat_h, slat), (sgain_h, sgain), (rkey_h, rkey), (freq_h, freq),
         (qlat_h, qlat), (qgain_h, qgain), (qp_h, qp_w), (qt_h, qt_w),
         (gate_h.at[0], gate_w), (up_h.at[0], up_w), (down_h.at[0], down_w),
         (kw_h, key_w), (vw_h, value_w), (mw_h, mixer_w),
@@ -676,64 +678,6 @@
     def landed(copy, when):
         pl.when(when)(copy.wait_recv)
 
-    ready(0, 2)
-    expert = lax.broadcasted_iota(jnp.int32, (n_ep, tokens), 0)
-    member = jnp.zeros((n_ep, tokens), F32)
-    weight = jnp.zeros((n_ep, tokens), F32)
-    for k in range(routing.shape[0]):
-        named = routing[k : k + 1, :] == expert
-        member = member + jnp.where(named, 1.0, 0.0)
-        weight = weight + jnp.where(named, share[k : k + 1, :], 0.0)
-    before = lax.broadcasted_iota(jnp.int32, (tokens, tokens), 0) < lax.broadcasted_iota(
-        jnp.int32, (tokens, tokens), 1
-    )
-    placed = jnp.dot(
-        member.astype(BF16),
-        jnp.where(before, 1.0, 0.0).astype(BF16),
-        preferred_element_type=F32,
-    )
-    placed = jnp.where(member > 0.0, placed, -1.0)
-    ranks[...] = placed
-    ready(2, 4)
-    normed[...] = norm_rows(ein[...], egain[...][None, :])
-    slot_row = lax.broadcasted_iota(jnp.int32, (capacity, tokens), 0).astype(F32)
-
-    def chosen(e):
-        return jnp.where(ranks[pl.ds(e, 1), :] == slot_row, 1.0, 0.0).astype(BF16)
-
-    own_cols = normed[:, cols(me_t)]
-    for d in range(depth):
-        for f in range(2):
-            if d or f:
-                disp[2 * d + f] = jnp.dot(
-                    chosen(ep_at(d, f)), own_cols, preferred_element_type=F32
-                ).astype(BF16)
-    pl.semaphore_wait(barrier, len(peers))
-
-    def disp_at(i, t):
-        return arr.at[i, :, cols(t)]
-
-    def direct(i):
-        return remote(
-            disp.at[i], disp_at(i, me_t), d_s.at[i], d_r.at[i], ep_at(i // 2, i % 2), me_t
-        )
-
-    spread = [1, depth - 1] + list(range(2, depth - 1))
-    go(direct(1))
-    for f in range(2):
-        go(direct(2 * spread[0] + f))
-
-    ready(4, 8)
-    position = lax.broadcasted_iota(jnp.int32, (rows, LANES), 0) + me_e * rows
-    angles = position.astype(F32) * freq[...]
-    cosine = jnp.cos(angles)
-    sine = jnp.sin(angles)
-    latent = norm_rows(slat[...], sgain[...][None, :])
-    lat_all[0, :, :rank] = latent
-    key_rows = jnp.transpose(rkey[...].astype(F32))
-    lat_all[0, :, rank:] = turn_pair(
-        jnp.concatenate([key_rows, key_rows], axis=1), cosine, sine
-    ).astype(BF16)
     lat_rows = rows // CORES
 
     def lat_at(i, core):
@@ -759,11 +703,6 @@
     def known(i):
         return x == 1 if i == 1 else z >= i // 2
 
-    go(lat_x(0), x == 0)
-    lat_up(0)
-    for d in spread[1:]:
-        for f in range(2):
-            go(direct(2 * d + f))
 
     def z_arr(d):
         landed(lat_z(d), known(2 * d))
@@ -775,28 +714,21 @@
         landed(lat_x(d), known(2 * d + 1))
         go(lat_c(2 * d + 1, c), known(2 * d + 1))
 
-    arr[0] = jnp.dot(chosen(me_e), normed[...], preferred_element_type=F32).astype(BF16)
-    placed_t = jnp.transpose(placed)
-    weight_t = jnp.transpose(weight)
-    lane = lax.broadcasted_iota(jnp.int32, (tokens, n_ep), 1)
-    slot_col = lax.broadcasted_iota(jnp.int32, (tokens, capacity), 1).astype(F32)
-    for i in range(n_ep):
-        mine = lane == ep_at(i // 2, i % 2)
-        place = jnp.sum(jnp.where(mine, placed_t, 0.0), axis=1, keepdims=True)
-        scale = jnp.sum(jnp.where(mine, weight_t, 0.0), axis=1, keepdims=True)
-        mixing[i] = jnp.where(place == slot_col, scale, 0.0)
-
-    ready(8, 12)
-    query = norm_rows(qlat[...], qgain[...][None, :])
-    plain = jnp.dot(query, qp_w[...], preferred_element_type=F32).astype(BF16)
-    raw = jnp.dot(query, qt_w[...], preferred_element_type=F32)
-    group = lax.broadcasted_iota(jnp.int32, (rows, LANES), 1) // ROPE
-    for h in range(heads):
-        j = h * ROPE // LANES
-        turned = turn_pair(raw[:, j * LANES : (j + 1) * LANES], cosine, sine)
-        turned = jnp.where(group == h % (LANES // ROPE), turned, 0.0)
-        queries[:, h * head_keys : h * head_keys + NOPE] = plain[:, h * NOPE : (h + 1) * NOPE]
-        queries[:, h * head_keys + NOPE : (h + 1) * head_keys] = turned.astype(BF16)
+    def chosen(e):
+        return jnp.where(ranks[pl.ds(e, 1), :] == slot_row, 1.0, 0.0).astype(BF16)
+
+    def disp_at(i, t):
+        return arr.at[i, :, cols(t)]
+
+    def direct(i):
+        return remote(
+            disp.at[i], disp_at(i, me_t), d_s.at[i], d_r.at[i], ep_at(i // 2, i % 2), me_t
+        )
+
+    kept = []
+
+    def keep(src, dst, at):
+        kept.append(take(src.at[at], dst.at[at], keep_sem.at[len(kept)]))
 
     def relay(i):
         direct(i).wait_recv()
@@ -948,102 +880,205 @@
         ref = mout.at[mix_rows(n), side(core)]
         return remote(ref, ref, mo_s.at[n], mo_r.at[n], me_e, mate)
 
-    first, second, third = (2 * d for d in spread)
+    def mixer_turn(n):
+        mixer_core(n).wait_recv()
+        at = mix_rows(n)
+        msum[at] = (mown[at] + mca[at].astype(F32)).astype(BF16)
+        go(mixer_y(n))
+
+    def mixer_end(n):
+        mixer_y(n).wait_recv()
+        at = mix_rows(n)
+        mout[at, side(c)] = (msum[at].astype(F32) + mya[at].astype(F32)).astype(BF16)
+        go(mixer_out(n, c))
+        keep(mout, mout_h, (mix_rows(n), side(c)))
+
     middle = n_ep // 2
+    ready(4, 6)
+    expert = lax.broadcasted_iota(jnp.int32, (n_ep, tokens), 0)
+    member = jnp.zeros((n_ep, tokens), F32)
+    weight = jnp.zeros((n_ep, tokens), F32)
+    for k in range(routing.shape[0]):
+        named = routing[k : k + 1, :] == expert
+        member = member + jnp.where(named, 1.0, 0.0)
+        weight = weight + jnp.where(named, share[k : k + 1, :], 0.0)
+    before = lax.broadcasted_iota(jnp.int32, (tokens, tokens), 0) < lax.broadcasted_iota(
+        jnp.int32, (tokens, tokens), 1
+    )
+    placed = jnp.dot(
+        member.astype(BF16),
+        jnp.where(before, 1.0, 0.0).astype(BF16),
+        preferred_element_type=F32,
+    )
+    placed = jnp.where(member > 0.0, placed, -1.0)
+    ranks[...] = placed
+    ready(6, 8)
+    normed[...] = norm_rows(ein[...], egain[...][None, :])
+    slot_row = lax.broadcasted_iota(jnp.int32, (capacity, tokens), 0).astype(F32)
+
+    own_cols = normed[:, cols(me_t)]
+    for d in range(depth):
+        for f in range(2):
+            if d or f:
+                disp[2 * d + f] = jnp.dot(
+                    chosen(ep_at(d, f)), own_cols, preferred_element_type=F32
+                ).astype(BF16)
+    pl.semaphore_wait(barrier, len(peers))
+    go(direct(3))
+    ready(0, 4)
+    position = lax.broadcasted_iota(jnp.int32, (rows, LANES), 0) + me_e * rows
+    angles = position.astype(F32) * freq[...]
+    cosine = jnp.cos(angles)
+    sine = jnp.sin(angles)
+    latent = norm_rows(slat[...], sgain[...][None, :])
+    lat_all[0, :, :rank] = latent
+    key_rows = jnp.transpose(rkey[...].astype(F32))
+    lat_all[0, :, rank:] = turn_pair(
+        jnp.concatenate([key_rows, key_rows], axis=1), cosine, sine
+    ).astype(BF16)
+    go(direct(2))
+    go(direct(1))
     ready(15, 17)
     project(0)
+    lat_up(0)
+    go(direct(7))
     relay(1)
-    relay(first)
-    relay(first + 1)
+    relay(3)
+    go(lat_x(0), x == 0)
+    go(direct(6))
     forward(1)
+    relay(2)
+    relay(7)
+    z_arr(1)
+    forward(3)
     x_arr(0)
-    z_arr(1)
+    forward(2)
+    relay(6)
     arrive(1)
+    lat_arrive(2)
+    go(direct(5))
+    arr[0] = jnp.dot(chosen(me_e), normed[...], preferred_element_type=F32).astype(BF16)
+    placed_t = jnp.transpose(placed)
+    weight_t = jnp.transpose(weight)
+    lane = lax.broadcasted_iota(jnp.int32, (tokens, n_ep), 1)
+    slot_col = lax.broadcasted_iota(jnp.int32, (tokens, capacity), 1).astype(F32)
+    for i in range(n_ep):
+        mine = lane == ep_at(i // 2, i % 2)
+        place = jnp.sum(jnp.where(mine, placed_t, 0.0), axis=1, keepdims=True)
+        scale = jnp.sum(jnp.where(mine, weight_t, 0.0), axis=1, keepdims=True)
+        mixing[i] = jnp.where(place == slot_col, scale, 0.0)
+
+    arrive(3)
     ready(12, 15)
     chunk(0)
-    forward(first)
-    forward(first + 1)
-    relay(second)
-    relay(second + 1)
-    y_step(0)
+    z_arr(2)
+    arrive(2)
+    chunk(1)
     y_step(1)
-    z_arr(2)
+    lat_arrive(1)
+    forward(7)
     x_arr(1)
-    arrive(first)
-    arrive(first + 1)
-    chunk(first // 2)
-    lat_arrive(1)
+    go(direct(4))
     project(1)
-    forward(second)
-    forward(second + 1)
-    relay(third)
-    relay(third + 1)
+    y_step(2)
+    ready(8, 12)
+    query = norm_rows(qlat[...], qgain[...][None, :])
+    plain = jnp.dot(query, qp_w[...], preferred_element_type=F32).astype(BF16)
+    raw = jnp.dot(query, qt_w[...], preferred_element_type=F32)
+    group = lax.broadcasted_iota(jnp.int32, (rows, LANES), 1) // ROPE
+    for h in range(heads):
+        j = h * ROPE // LANES
+        turned = turn_pair(raw[:, j * LANES : (j + 1) * LANES], cosine, sine)
+        turned = jnp.where(group == h % (LANES // ROPE), turned, 0.0)
+        queries[:, h * head_keys : h * head_keys + NOPE] = plain[:, h * NOPE : (h + 1) * NOPE]
+        queries[:, h * head_keys + NOPE : (h + 1) * head_keys] = turned.astype(BF16)
+
+    lat_arrive(3)
+    forward(6)
+    arrive(7)
+    project(2)
+    arrive(6)
+    project(3)
+    sum_step(1)
+    lat_arrive(4)
+    relay(5)
+    chunk(3)
+    relay(4)
     z_arr(3)
     x_arr(2)
-    y_step(first)
-    y_step(first + 1)
-    sum_step(0)
-    sum_step(1)
-    arrive(second)
-    arrive(second + 1)
-    chunk(second // 2)
-    for i in range(2, middle):
-        lat_arrive(i)
-        project(i)
-    forward(third)
-    forward(third + 1)
+    attend(0, 0, middle)
+    project(4)
+    forward(5)
+    y_step(3)
+    sum_step(2)
+    y_step(7)
+    attend(2, 0, middle)
+    lat_arrive(6)
+    mix(1)
+    attend(3, 0, middle)
+    y_step(6)
+    lat_arrive(5)
+    project(6)
+    forward(4)
+    project(5)
+    attend(1, 0, middle)
+    arrive(4)
+    y_step(0)
+    arrive(5)
     x_arr(3)
-    y_step(second)
-    y_step(second + 1)
-    sum_step(first)
-    sum_step(first + 1)
-    for h in range(heads // 2):
-        attend(h, 0, middle)
-    arrive(third)
-    arrive(third + 1)
-    chunk(third // 2)
-    for h in range(heads // 2, heads):
-        attend(h, 0, middle)
-    y_step(third)
-    y_step(third + 1)
-    for i in range(middle, n_ep):
-        lat_arrive(i)
-        project(i)
-    sum_step(second)
-    sum_step(second + 1)
-    for h in range(heads):
-        attend(h, middle, n_ep)
+    chunk(2)
+    sum_step(3)
+    lat_arrive(7)
+    project(7)
+    attend(3, middle, n_ep)
+    attend(0, middle, n_ep)
+    y_step(5)
+    attend(2, middle, n_ep)
+    sum_step(7)
+    sum_step(6)
+    y_step(4)
+    attend(1, middle, n_ep)
     ready(17, 18)
     msend[...] = jnp.dot(
         out[...], mixer_w[:, side(1 - c)], preferred_element_type=F32
     ).astype(BF16)
     for n in range(pieces):
         go(mixer_core(n))
+    sum_step(0)
     mown[...] = jnp.dot(out[...], mixer_w[:, side(c)], preferred_element_type=F32)
-    sum_step(third)
-    sum_step(third + 1)
-    for n in range(pieces):
-        mixer_core(n).wait_recv()
-        at = mix_rows(n)
-        msum[at] = (mown[at] + mca[at].astype(F32)).astype(BF16)
-        go(mixer_y(n))
-    for i in (0, first, second, third):
-        mix(i)
-        mix(i + 1)
+    sum_step(5)
+    mixer_turn(0)
+    mixer_turn(3)
+    sum_step(4)
+    mix(2)
+    mixer_turn(1)
+    mix(6)
+    mix(7)
+    mix(0)
+    mixer_turn(2)
+    mix(3)
+    mix(5)
+    mixer_end(1)
+    mix(4)
     eout[:, cols(me_t)] = acc[0].astype(BF16)
     go(out_copy(0, me_t, over))
     go(out_copy(1, me_t, mate))
-    for n in range(pieces):
-        mixer_y(n).wait_recv()
-        at = mix_rows(n)
-        mout[at, side(c)] = (msum[at].astype(F32) + mya[at].astype(F32)).astype(BF16)
-        go(mixer_out(n, c))
+    keep(eout, eout_h, (slice(None), cols(me_t)))
+    mixer_end(0)
+    mixer_end(3)
+    mixer_end(2)
     out_copy(0, over, over).wait_recv()
     go(out_copy(2, over, mate))
-    out_copy(1, mate, mate).wait_recv()
-    out_copy(2, far, mate).wait_recv()
+    keep(eout, eout_h, (slice(None), cols(over)))
     for n in range(pieces):
         mixer_out(n, 1 - c).wait_recv()
+        keep(mout, mout_h, (mix_rows(n), side(1 - c)))
+    out_copy(1, mate, mate).wait_recv()
+    keep(eout, eout_h, (slice(None), cols(mate)))
+    out_copy(2, far, mate).wait_recv()
+    keep(eout, eout_h, (slice(None), cols(far)))
+    for copy in kept:
+        copy.wait()
     for when, copy in sends:
         if when is None:
             copy.wait_send()
@@ -1116,8 +1151,13 @@
             jax.ShapeDtypeStruct((rows, width), BF16),
         ),
         in_specs=[pl.BlockSpec(memory_space=pltpu.HBM)] * len(args),
-        out_specs=vmem(2),
-        scratch_shapes=held
+        out_specs=[pl.BlockSpec(memory_space=pltpu.HBM)] * 2,
+        scratch_shapes=[
+            pltpu.VMEM((tokens, width), BF16),
+            pltpu.VMEM((rows, width), BF16),
+            dma((12,)),
+        ]
+        + held
         + [
             dma((len(args),)),
             pltpu.VMEM((tokens, width), BF16),
@@ -1178,7 +1218,33 @@
             collective_id=2, has_side_effects=True, vmem_limit_bytes=FUSED_LIMIT
         ),
     )(*args)
-    return (mixer_output, expert_output)
+    results = (mixer_output, expert_output)
+    return tuple(
+        pl.pallas_call(
+            settle,
+            out_shape=tuple(jax.ShapeDtypeStruct(r.shape, r.dtype) for r in results),
+            in_specs=[pl.BlockSpec(memory_space=pltpu.HBM)] * 2,
+            out_specs=[pl.BlockSpec(memory_space=pltpu.HBM)] * 2,
+            scratch_shapes=[pltpu.VMEM(r.shape, r.dtype) for r in results]
+            + [dma((2, PARTS)), dma((2, PARTS))],
+        )(*results)
+    )
+
+
+def settle(first_in, second_in, first_out, second_out, first_held, second_held, in_sem, out_sem):
+    arrays = ((first_in, first_held, first_out), (second_in, second_held, second_out))
+    coming = []
+    for j, (src, held, dst) in enumerate(arrays):
+        step = held.shape[0] // PARTS
+        for n in range(PARTS):
+            at = slice(n * step, (n + 1) * step)
+            coming.append((take(src.at[at], held.at[at], in_sem.at[j, n]), held, dst, at, j, n))
+    leaving = []
+    for copy, held, dst, at, j, n in coming:
+        copy.wait()
+        leaving.append(take(held.at[at], dst.at[at], out_sem.at[j, n]))
+    for copy in leaving:
+        copy.wait()
 
 
 def pick(mesh):

time: 76 us -> 67.4 us (0.89)
  Pallas kernels: 72 us -> 65.9 us
  local copies, waits for them, and re-layouts: 3.16 us -> 0 us
    pallas_call x1, Pallas kernels: 72 us -> 63.7 us  [fused(): pl.pallas_call(functools.partial(step_kernel, n_ep, n_tp, heads), out_sha...]
    unnamed x4 -> x0, local copies, waits for them, and re-layouts: 3.16 us -> none
    pallas_call x0 -> x1, Pallas kernels: none -> 2.22 us  [fused(): pl.pallas_call(settle, out_shape=tuple((jax.ShapeDtypeStruct(r.shape, r.d...]
where the time goes in v3:
time: 67.4 us; the launch traced here: 66.7 us
  Pallas kernels  65.9 us (98%)
  between operations  0.81 us (1%)
    pallas_call x1, Pallas kernels, fused(): pl.pallas_call(functools.partial(step_kernel, n_ep, n_tp, heads), out_sha...  63.7 us
    pallas_call x1, Pallas kernels, fused(): pl.pallas_call(settle, out_shape=tuple((jax.ShapeDtypeStruct(r.shape, r.d...  2.22 us

profile of v3, /device:TPU:0, one launch (start us, length us, event | category | flops | bytes accessed | tf_op | source)
XLA Modules:
  0.0 66.7 jit_solution(11313253953734032963)
XLA Ops:
  0.6 63.7 %shard_map.185 = (bf16[128,2048]{1,0:T(8,128)(2,1)}, bf16[256,2048]{1,0:T(8,128)(2,1)}) custom-call(s32[4,128]{1,0:T(4,128)} %bitcast.4, f32[4,128]{1,0:T(4,128)} %bitcast.5, bf16[128,2048]{1,0:T(8,128)(2,1)} %refs_2_.1, f32[2048]{0:T(1024)} %refs_3_.1, bf16[256,512]{1,0:T(8,128)(2,1)} %refs_4_.1, f32[512]{0:T(512)} %refs_5_.1, bf16[64,256]{1,0:T(8,128)(2,1)} %bitcast.3, ...), custom_call_target="tpu_custom_call" | custom-call | tf_op jit(solution)/shard_map/pallas_call | solution.py:1147
  64.3 2.2 %shard_map.186 = (bf16[256,2048]{1,0:T(8,128)(2,1)}, bf16[128,2048]{1,0:T(8,128)(2,1)}) custom-call(bf16[256,2048]{1,0:T(8,128)(2,1)} %get-tuple-element.4.first_in, bf16[128,2048]{1,0:T(8,128)(2,1)} %get-tuple-element.5.second_in), custom_call_target="tpu_custom_call" | custom-call | tf_op jit(solution)/shard_map/pallas_call | solution.py:1223

commit v4 on v3

--- a/solution.py
+++ b/solution.py
@@ -938,25 +938,6 @@
     ).astype(BF16)
     go(direct(2))
     go(direct(1))
-    ready(15, 17)
-    project(0)
-    lat_up(0)
-    go(direct(7))
-    relay(1)
-    relay(3)
-    go(lat_x(0), x == 0)
-    go(direct(6))
-    forward(1)
-    relay(2)
-    relay(7)
-    z_arr(1)
-    forward(3)
-    x_arr(0)
-    forward(2)
-    relay(6)
-    arrive(1)
-    lat_arrive(2)
-    go(direct(5))
     arr[0] = jnp.dot(chosen(me_e), normed[...], preferred_element_type=F32).astype(BF16)
     placed_t = jnp.transpose(placed)
     weight_t = jnp.transpose(weight)
@@ -968,19 +949,44 @@
         scale = jnp.sum(jnp.where(mine, weight_t, 0.0), axis=1, keepdims=True)
         mixing[i] = jnp.where(place == slot_col, scale, 0.0)
 
-    arrive(3)
+    go(direct(7))
+    lat_up(0)
+    relay(3)
+    relay(1)
+    go(lat_x(0), x == 0)
+    relay(2)
+    go(direct(6))
+    forward(1)
+    forward(3)
+    z_arr(1)
+    relay(7)
+    arrive(1)
+    ready(15, 17)
+    project(0)
+    relay(6)
+    forward(2)
     ready(12, 15)
     chunk(0)
+    go(direct(5))
+    x_arr(1)
+    forward(7)
+    y_step(0)
     z_arr(2)
     arrive(2)
+    y_step(1)
+    arrive(7)
+    arrive(3)
     chunk(1)
-    y_step(1)
+    lat_arrive(3)
+    x_arr(0)
+    go(direct(4))
+    project(3)
+    forward(6)
+    lat_arrive(2)
+    project(2)
+    y_step(3)
     lat_arrive(1)
-    forward(7)
-    x_arr(1)
-    go(direct(4))
-    project(1)
-    y_step(2)
+    relay(5)
     ready(8, 12)
     query = norm_rows(qlat[...], qgain[...][None, :])
     plain = jnp.dot(query, qp_w[...], preferred_element_type=F32).astype(BF16)
@@ -993,86 +999,80 @@
         queries[:, h * head_keys : h * head_keys + NOPE] = plain[:, h * NOPE : (h + 1) * NOPE]
         queries[:, h * head_keys + NOPE : (h + 1) * head_keys] = turned.astype(BF16)
 
-    lat_arrive(3)
-    forward(6)
-    arrive(7)
-    project(2)
+    project(1)
+    z_arr(3)
     arrive(6)
-    project(3)
-    sum_step(1)
+    attend(1, 0, middle)
+    chunk(3)
+    x_arr(2)
+    relay(4)
+    y_step(2)
+    attend(2, 0, middle)
+    forward(5)
+    y_step(6)
     lat_arrive(4)
-    relay(5)
-    chunk(3)
-    relay(4)
-    z_arr(3)
-    x_arr(2)
+    attend(3, 0, middle)
+    lat_arrive(5)
+    sum_step(3)
     attend(0, 0, middle)
+    lat_arrive(6)
+    x_arr(3)
     project(4)
-    forward(5)
-    y_step(3)
-    sum_step(2)
-    y_step(7)
-    attend(2, 0, middle)
-    lat_arrive(6)
-    mix(1)
-    attend(3, 0, middle)
-    y_step(6)
-    lat_arrive(5)
     project(6)
     forward(4)
     project(5)
-    attend(1, 0, middle)
+    lat_arrive(7)
+    arrive(5)
+    project(7)
+    attend(2, middle, n_ep)
+    y_step(7)
+    sum_step(2)
     arrive(4)
-    y_step(0)
-    arrive(5)
-    x_arr(3)
     chunk(2)
-    sum_step(3)
-    lat_arrive(7)
-    project(7)
     attend(3, middle, n_ep)
-    attend(0, middle, n_ep)
-    y_step(5)
-    attend(2, middle, n_ep)
-    sum_step(7)
+    sum_step(0)
     sum_step(6)
+    mix(3)
     y_step(4)
     attend(1, middle, n_ep)
+    attend(0, middle, n_ep)
+    sum_step(7)
+    y_step(5)
     ready(17, 18)
     msend[...] = jnp.dot(
         out[...], mixer_w[:, side(1 - c)], preferred_element_type=F32
     ).astype(BF16)
     for n in range(pieces):
         go(mixer_core(n))
-    sum_step(0)
+    sum_step(1)
     mown[...] = jnp.dot(out[...], mixer_w[:, side(c)], preferred_element_type=F32)
+    sum_step(4)
+    mixer_turn(0)
+    mix(6)
+    mixer_turn(3)
+    mix(2)
+    mix(0)
+    mixer_turn(1)
+    mix(7)
     sum_step(5)
-    mixer_turn(0)
-    mixer_turn(3)
-    sum_step(4)
-    mix(2)
-    mixer_turn(1)
-    mix(6)
-    mix(7)
-    mix(0)
     mixer_turn(2)
-    mix(3)
+    mix(4)
+    mixer_end(3)
+    mixer_end(1)
     mix(5)
-    mixer_end(1)
-    mix(4)
+    mix(1)
+    mixer_end(0)
     eout[:, cols(me_t)] = acc[0].astype(BF16)
     go(out_copy(0, me_t, over))
     go(out_copy(1, me_t, mate))
     keep(eout, eout_h, (slice(None), cols(me_t)))
-    mixer_end(0)
-    mixer_end(3)
     mixer_end(2)
+    for n in range(pieces):
+        mixer_out(n, 1 - c).wait_recv()
+        keep(mout, mout_h, (mix_rows(n), side(1 - c)))
     out_copy(0, over, over).wait_recv()
     go(out_copy(2, over, mate))
     keep(eout, eout_h, (slice(None), cols(over)))
-    for n in range(pieces):
-        mixer_out(n, 1 - c).wait_recv()
-        keep(mout, mout_h, (mix_rows(n), side(1 - c)))
     out_copy(1, mate, mate).wait_recv()
     keep(eout, eout_h, (slice(None), cols(mate)))
     out_copy(2, far, mate).wait_recv()

time: 67.4 us -> 68.6 us (1.018)
  Pallas kernels: 65.9 us -> 67 us
    pallas_call x1, Pallas kernels: 63.7 us -> 64.7 us  [fused(): pl.pallas_call(functools.partial(step_kernel, n_ep, n_tp, heads), out_sha...]
where the time goes in v4:
time: 68.6 us; the launch traced here: 67.8 us
  Pallas kernels  67 us (98%)
  between operations  0.81 us (1%)
    pallas_call x1, Pallas kernels, fused(): pl.pallas_call(functools.partial(step_kernel, n_ep, n_tp, heads), out_sha...  64.7 us
    pallas_call x1, Pallas kernels, fused(): pl.pallas_call(settle, out_shape=tuple((jax.ShapeDtypeStruct(r.shape, r.d...  2.22 us

profile of v4, /device:TPU:0, one launch (start us, length us, event | category | flops | bytes accessed | tf_op | source)
XLA Modules:
  0.0 67.8 jit_solution(10143402977960040510)
XLA Ops:
  0.6 64.7 %shard_map.185 = (bf16[128,2048]{1,0:T(8,128)(2,1)}, bf16[256,2048]{1,0:T(8,128)(2,1)}) custom-call(s32[4,128]{1,0:T(4,128)} %bitcast.4, f32[4,128]{1,0:T(4,128)} %bitcast.5, bf16[128,2048]{1,0:T(8,128)(2,1)} %refs_2_.1, f32[2048]{0:T(1024)} %refs_3_.1, bf16[256,512]{1,0:T(8,128)(2,1)} %refs_4_.1, f32[512]{0:T(512)} %refs_5_.1, bf16[64,256]{1,0:T(8,128)(2,1)} %bitcast.3, ...), custom_call_target="tpu_custom_call" | custom-call | tf_op jit(solution)/shard_map/pallas_call | solution.py:1147
  65.4 2.2 %shard_map.186 = (bf16[256,2048]{1,0:T(8,128)(2,1)}, bf16[128,2048]{1,0:T(8,128)(2,1)}) custom-call(bf16[256,2048]{1,0:T(8,128)(2,1)} %get-tuple-element.4.first_in, bf16[128,2048]{1,0:T(8,128)(2,1)} %get-tuple-element.5.second_in), custom_call_target="tpu_custom_call" | custom-call | tf_op jit(solution)/shard_map/pallas_call | solution.py:1223
